TPU v7x, 32 devices: a whole 2x2x4 slice. The times are simulated.
32 devices in a mesh: sp: 8 (over z, x), dp: 4 (over y, core).
Axes of the slice: x: 2, y: 2, z: 4, core: 2. Of those that a mesh axis runs over, the one named last changes fastest.
Arguments:
- layer_activity: bfloat16 [4, 1024, 2048], P('dp', 'sp'), may hold values from -6 to 6
- writer_matrix: bfloat16 [2048, 256], P('dp'), may hold values from -0.125 to 0.125
- reader_matrix: bfloat16 [2048, 256], P('dp'), may hold values from -0.125 to 0.125
- source_unfiltered: bfloat16 [4, 1024, 2048], P('dp', 'sp'), may hold values from -6 to 6
- switch_raw_signal: bfloat16 [4, 1024, 2048], P('dp', 'sp'), may hold values from -6 to 6
- saved_result: bfloat16 [4, 1024, 2048], P('dp', 'sp'), may hold values from -6 to 6
- final_adjoint: bfloat16 [4, 1024, 2048], P('dp', 'sp'), may hold values from -6 to 6
- delta_raw: bfloat16 [4, 1024, 32], P('dp', 'sp'), may hold values from -4 to 4
- extra_logdrop: float32 [4, 1024, 32], P('dp', None, 'sp'), may hold values from 0 to 2.1
- source_filter_coefs: float32 [5, 2048], P(None, 'sp'), may hold values from -2.5 to 2.5
- writer_filter_coefs: float32 [5, 256], replicated, may hold values from -2.5 to 2.5
- reader_filter_coefs: float32 [5, 256], replicated, may hold values from -2.5 to 2.5
- delta_offset: float32 [32], P('sp'), may hold values from -7.5 to -6
- fading_exponents: float32 [32], P('sp'), may hold values from -6 to 3.4
- direct_factor: float32 [32], P('sp'), may hold values from 0.1 to 1.9
- rescale_factor: float32 [2048], replicated, may hold values from 0.1 to 1.9
Outputs:
- d_hidden: bfloat16 [4, 1024, 2048], P('dp', 'sp')
- d_x_raw: bfloat16 [4, 1024, 2048], P('dp', 'sp')
- d_gate: bfloat16 [4, 1024, 2048], P('dp', 'sp')
- d_dt_raw: bfloat16 [4, 1024, 32], P('dp', 'sp')
- d_w_b: float32 [2048, 256], P('dp')
- d_w_c: float32 [2048, 256], P('dp')
All inputs are finite; a program needn't handle non-finite values.
Results may differ from a plain program's by a relative error of at most 0.012.
Values may be sent and summed in bfloat16 or wider, within the bound.
A program may use at most 128 MiB of HBM per device.

v0:
```python
import jax
import jax.numpy as jnp
from jax import lax
from jax.sharding import PartitionSpec as P

HEADS = 32
HEAD_DIM = 64
STATE = 128
GROUPS = 2
NORM_GROUPS = 8
CONV_K = 5
BLOCK = 128
INNER = 2048


EPSILON = 1e-06
highest = lax.Precision.HIGHEST


def centred_conv(values, tap_weights):
    sample_window = values.shape[0]
    reach_side = (tap_weights.shape[0] - 1) // 2
    padded = jnp.pad(values, ((reach_side, reach_side), (0, 0)))
    summed = jnp.zeros_like(values)
    for offset in range(tap_weights.shape[0]):
        summed = summed + tap_weights[offset][None, :] * padded[offset : offset + sample_window]
    return summed


def one_channel_scan(
    source_unfiltered,
    writer_unfiltered,
    reader_unfiltered,
    delta_raw,
    extra_logdrop,
    source_filter_coefs,
    writer_filter_coefs,
    reader_filter_coefs,
    delta_offset,
    fading_exponents,
    direct_factor,
):
    inputs = jax.nn.silu(centred_conv(source_unfiltered, source_filter_coefs))
    keys_b = jax.nn.silu(centred_conv(writer_unfiltered, writer_filter_coefs))
    reads_c = jax.nn.silu(centred_conv(reader_unfiltered, reader_filter_coefs))
    smooth_delta = jax.nn.softplus(delta_raw + delta_offset)
    channel_fading = smooth_delta * jnp.exp(fading_exponents) + extra_logdrop
    cumulative = jnp.cumsum(channel_fading)
    sample_window = source_unfiltered.shape[0]
    blocks = sample_window // BLOCK
    driven = (inputs * smooth_delta[:, None]).reshape(blocks, BLOCK, -1)
    keyed = keys_b.reshape(blocks, BLOCK, -1)
    reading = reads_c.reshape(blocks, BLOCK, -1)
    levels = cumulative.reshape(blocks, BLOCK)
    within = jnp.exp(-jnp.abs(levels[:, :, None] - levels[:, None, :]))
    scores = jnp.einsum("ktn,ksn->kts", reading, keyed, precision=highest) * within
    output = jnp.einsum("kts,ksp->ktp", scores, driven, precision=highest)
    block_ends = levels[:, -1]
    block_starts = levels[:, 0]
    block_order = jnp.arange(blocks, dtype=jnp.int32)
    prev_end = jnp.concatenate([cumulative[:1], block_ends[:-1]])
    next_start = jnp.concatenate([block_starts[1:], cumulative[-1:]])
    weight_fwd = jnp.exp(levels - block_ends[:, None])
    state_fwd = jnp.einsum(
        "ksn,ksp->knp", keyed * weight_fwd[:, :, None], driven, precision=highest
    )
    mask_fwd = (block_order[None, :] < block_order[:, None]).astype(cumulative.dtype)
    link_fwd = jnp.exp(-jnp.abs(prev_end[:, None] - block_ends[None, :])) * mask_fwd
    carry_fwd = jnp.einsum("kj,jnp->knp", link_fwd, state_fwd, precision=highest)
    read_fwd = reading * jnp.exp(prev_end[:, None] - levels)[:, :, None]
    weight_bwd = jnp.exp(block_starts[:, None] - levels)
    state_bwd = jnp.einsum(
        "ksn,ksp->knp", keyed * weight_bwd[:, :, None], driven, precision=highest
    )
    mask_bwd = (block_order[None, :] > block_order[:, None]).astype(cumulative.dtype)
    link_bwd = jnp.exp(-jnp.abs(next_start[:, None] - block_starts[None, :])) * mask_bwd
    carry_bwd = jnp.einsum("kj,jnp->knp", link_bwd, state_bwd, precision=highest)
    read_bwd = reading * jnp.exp(levels - next_start[:, None])[:, :, None]
    output = output + jnp.einsum("ktn,knp->ktp", read_fwd, carry_fwd, precision=highest)
    output = output + jnp.einsum("ktn,knp->ktp", read_bwd, carry_bwd, precision=highest)
    return output.reshape(sample_window, -1) + direct_factor * inputs


def channelwise_derivs(
    source_unfiltered,
    writer_unfiltered,
    reader_unfiltered,
    delta_raw,
    extra_logdrop,
    source_filter_coefs,
    writer_filter_coefs,
    reader_filter_coefs,
    delta_offset,
    fading_exponents,
    direct_factor,
    result_adjoint,
):

    def forward(source_filtered, writer_filtered, reader_filtered, delta_argument):
        return one_channel_scan(
            source_filtered,
            writer_filtered,
            reader_filtered,
            delta_argument,
            extra_logdrop,
            source_filter_coefs,
            writer_filter_coefs,
            reader_filter_coefs,
            delta_offset,
            fading_exponents,
            direct_factor,
        )

    primal, pullback = jax.vjp(
        forward,
        source_unfiltered.astype(jnp.float32),
        writer_unfiltered.astype(jnp.float32),
        reader_unfiltered.astype(jnp.float32),
        delta_raw.astype(jnp.float32),
    )
    source_derivative, writer_derivative, reader_derivative, delta_derivative = pullback(
        result_adjoint.astype(jnp.float32)
    )
    return (
        source_derivative.astype(jnp.bfloat16),
        writer_derivative.astype(jnp.bfloat16),
        reader_derivative.astype(jnp.bfloat16),
        delta_derivative.astype(jnp.bfloat16),
    )


def gated_norm(values, gating, rescale_factor):
    mixed = values * jax.nn.silu(gating)
    grouped = mixed.reshape(mixed.shape[0], NORM_GROUPS, -1)
    scaled = grouped * lax.rsqrt(jnp.mean(grouped * grouped, axis=-1, keepdims=True) + EPSILON)
    return scaled.reshape(mixed.shape) * rescale_factor


def norm_backward(saved_result, switch_raw_signal, final_adjoint, rescale_factor):
    primal, pullback = jax.vjp(
        lambda values, gating: gated_norm(values, gating, rescale_factor),
        saved_result.astype(jnp.float32),
        switch_raw_signal.astype(jnp.float32),
    )
    d_values, d_gates = pullback(final_adjoint.astype(jnp.float32))
    return (d_values.astype(jnp.bfloat16), d_gates.astype(jnp.bfloat16))


def spread_heads(columns, tokens):
    grouped = columns.reshape(tokens, GROUPS, 1, STATE)
    copied = jnp.broadcast_to(grouped, (tokens, GROUPS, HEADS // GROUPS, STATE))
    return copied.reshape(1, tokens, HEADS * STATE)


def heads_first(values, window, local_channels, width):
    return jnp.transpose(values.reshape(window, local_channels, width), (1, 0, 2))


def local(
    layer_activity,
    writer_matrix,
    reader_matrix,
    source_unfiltered,
    switch_raw_signal,
    saved_result,
    final_adjoint,
    delta_raw,
    extra_logdrop,
    source_filter_coefs,
    writer_filter_coefs,
    reader_filter_coefs,
    delta_offset,
    fading_exponents,
    direct_factor,
    rescale_factor,
):
    tokens = layer_activity.shape[1]
    width_in = layer_activity.shape[2]
    latent_dimension = GROUPS * STATE
    data_devices = lax.axis_size("dp")
    local_channels = delta_offset.shape[0]
    per_group = HEADS // GROUPS
    weights = lax.all_gather(
        jnp.concatenate([writer_matrix, reader_matrix], axis=1), "dp", axis=0, tiled=True
    )
    token_rows = layer_activity.reshape(tokens, width_in)
    projected = jnp.dot(token_rows, weights, preferred_element_type=jnp.float32).astype(
        jnp.bfloat16
    )
    result_adjoint, d_gate = norm_backward(
        saved_result.reshape(tokens, INNER),
        switch_raw_signal.reshape(tokens, INNER),
        final_adjoint.reshape(tokens, INNER),
        rescale_factor,
    )
    copies_b = spread_heads(projected[:, :latent_dimension], tokens)
    copies_c = spread_heads(projected[:, latent_dimension:], tokens)
    heads_x, heads_b, heads_c, heads_dt, heads_dy = (
        lax.all_to_all(source_unfiltered, "sp", split_axis=2, concat_axis=1, tiled=True),
        lax.all_to_all(copies_b, "sp", split_axis=2, concat_axis=1, tiled=True),
        lax.all_to_all(copies_c, "sp", split_axis=2, concat_axis=1, tiled=True),
        lax.all_to_all(delta_raw, "sp", split_axis=2, concat_axis=1, tiled=True),
        lax.all_to_all(
            result_adjoint.reshape(1, tokens, INNER), "sp", split_axis=2, concat_axis=1, tiled=True
        ),
    )
    window = heads_x.shape[1]
    first_head = lax.axis_index("sp") * local_channels
    head_ids = first_head + jnp.arange(local_channels, dtype=jnp.int32)
    chooser = (
        head_ids[:, None] // per_group == jnp.arange(GROUPS, dtype=jnp.int32)[None, :]
    ).astype(jnp.float32)
    writer_filter_fn = jnp.einsum(
        "kgn,hg->hkn",
        writer_filter_coefs.reshape(CONV_K, GROUPS, STATE),
        chooser,
        precision=highest,
    )
    reader_filter_fn = jnp.einsum(
        "kgn,hg->hkn",
        reader_filter_coefs.reshape(CONV_K, GROUPS, STATE),
        chooser,
        precision=highest,
    )
    source_filter_fn = jnp.transpose(
        source_filter_coefs.reshape(CONV_K, local_channels, HEAD_DIM), (1, 0, 2)
    )
    per_head = jax.vmap(channelwise_derivs)
    source_derivative, writer_derivative, reader_derivative, delta_derivative = per_head(
        heads_first(heads_x, window, local_channels, HEAD_DIM),
        heads_first(heads_b, window, local_channels, STATE),
        heads_first(heads_c, window, local_channels, STATE),
        heads_dt.reshape(window, local_channels).T,
        extra_logdrop.reshape(window, local_channels).T,
        source_filter_fn,
        writer_filter_fn,
        reader_filter_fn,
        delta_offset,
        fading_exponents,
        direct_factor,
        heads_first(heads_dy, window, local_channels, HEAD_DIM),
    )
    back_x, back_b, back_c, back_dt = (
        lax.all_to_all(
            jnp.transpose(source_derivative, (1, 0, 2)).reshape(
                1, window, local_channels * HEAD_DIM
            ),
            "sp",
            split_axis=1,
            concat_axis=2,
            tiled=True,
        ),
        lax.all_to_all(
            jnp.transpose(writer_derivative, (1, 0, 2)).reshape(1, window, local_channels * STATE),
            "sp",
            split_axis=1,
            concat_axis=2,
            tiled=True,
        ),
        lax.all_to_all(
            jnp.transpose(reader_derivative, (1, 0, 2)).reshape(1, window, local_channels * STATE),
            "sp",
            split_axis=1,
            concat_axis=2,
            tiled=True,
        ),
        lax.all_to_all(
            delta_derivative.T.reshape(1, window, local_channels),
            "sp",
            split_axis=1,
            concat_axis=2,
            tiled=True,
        ),
    )
    summed_b = jnp.sum(back_b.reshape(tokens, GROUPS, per_group, STATE).astype(jnp.float32), axis=2)
    summed_c = jnp.sum(back_c.reshape(tokens, GROUPS, per_group, STATE).astype(jnp.float32), axis=2)
    gradients = jnp.concatenate(
        [
            summed_b.reshape(tokens, latent_dimension).astype(jnp.bfloat16),
            summed_c.reshape(tokens, latent_dimension).astype(jnp.bfloat16),
        ],
        axis=1,
    )
    d_hidden = jnp.einsum(
        "tc,dc->td", gradients, weights, preferred_element_type=jnp.float32
    ).astype(jnp.bfloat16)
    column_block = lax.all_to_all(layer_activity, "dp", split_axis=2, concat_axis=0, tiled=True)
    all_columns = column_block.reshape(data_devices * tokens, width_in // data_devices)
    all_grads = lax.all_gather(gradients, "dp", axis=0, tiled=True)
    local_rows = jnp.einsum("td,tc->dc", all_columns, all_grads, preferred_element_type=jnp.float32)
    total_grad = lax.psum(local_rows, "sp")
    return (
        d_hidden.reshape(1, tokens, width_in),
        back_x,
        d_gate.reshape(1, tokens, INNER),
        back_dt,
        total_grad[:, :latent_dimension],
        total_grad[:, latent_dimension:],
    )


def solution(mesh):
    in_specs = (
        P("dp", "sp", None),
        P("dp", None),
        P("dp", None),
        P("dp", "sp", None),
        P("dp", "sp", None),
        P("dp", "sp", None),
        P("dp", "sp", None),
        P("dp", "sp", None),
        P("dp", None, "sp"),
        P(None, "sp"),
        P(),
        P(),
        P("sp"),
        P("sp"),
        P("sp"),
        P(),
    )
    out_specs = (
        P("dp", "sp", None),
        P("dp", "sp", None),
        P("dp", "sp", None),
        P("dp", "sp", None),
        P("dp", None),
        P("dp", None),
    )
    return jax.shard_map(local, mesh=mesh, in_specs=in_specs, out_specs=out_specs, check_vma=False)
```

profile of v0, /device:TPU:0, one launch (start us, length us, event | category | flops | bytes accessed | tf_op | source)
XLA Modules:
  0.0 509.0 jit_solution(16484277088458486737)
XLA Ops:
  11.6 7.3 %all-to-all-start.1 = ((bf16[8,2,256]{2,1,0:T(2,128)(2,1)}), bf16[8,2,256]{2,1,0:T(2,128)(2,1)S(1)}, u32[]{:S(2)}, u32[]{:S(2)}) async-start(bf16[8,2,256]{2,1,0:T(2,128)(2,1)} %reshape.408), calls=%async_computation.1 | async-start | bytes 16384 | tf_op jit(solution)/shard_map/all_to_all | solution.py:202
  21.4 11.6 %reduce.19 = bf16[2048,128]{1,0:T(8,128)(2,1)S(1)} reduce(bf16[2048,1,128]{2,1,0:T(2,128)(2,1)S(1)} %bitcast.410, bf16[]{:T(256)} %broadcast.265), dimensions={1}, to_apply=%bitcast.316.reduce_sub_computation | reduce | bytes 1048578
  33.8 3.5 all-to-all-start.9
  38.1 11.6 %reduce.14 = bf16[2048,128]{1,0:T(8,128)(2,1)S(1)} reduce(bf16[2048,1,128]{2,1,0:T(2,128)(2,1)S(1)} %bitcast.411, bf16[]{:T(256)} %broadcast.265), dimensions={1}, to_apply=%bitcast.304.reduce_sub_computation | reduce | bytes 1048578
  51.3 6.3 %all-to-all-start = ((bf16[8,2,16384]{2,1,0:T(2,128)(2,1)}), bf16[8,2,16384]{2,1,0:T(2,128)(2,1)}, u32[]{:S(2)}, u32[]{:S(2)}) async-start(bf16[8,2,16384]{2,1,0:T(2,128)(2,1)} %reshape.410), calls=%async_computation | async-start | bytes 1048576 | tf_op jit(solution)/shard_map/all_to_all | solution.py:199
  58.9 3.2 fusion.79
  64.4 11.6 %reduce.13 = bf16[2048,128]{1,0:T(8,128)(2,1)S(1)} reduce(bf16[2048,1,128]{2,1,0:T(2,128)(2,1)S(1)} %bitcast.407, bf16[]{:T(256)} %broadcast.265), dimensions={1}, to_apply=%bitcast.306.reduce_sub_computation | reduce | bytes 1048578
  76.9 6.3 %all-to-all-start.3 = ((bf16[8,2,16384]{2,1,0:T(2,128)(2,1)}), bf16[8,2,16384]{2,1,0:T(2,128)(2,1)}, u32[]{:S(2)}, u32[]{:S(2)}) async-start(bf16[8,2,16384]{2,1,0:T(2,128)(2,1)} %reshape.412), calls=%async_computation.3 | async-start | bytes 1048576 | tf_op jit(solution)/shard_map/all_to_all | solution.py:203
  86.1 16.7 %copy.538 = bf16[1,128,4096]{1,0,2:T(2,128)(2,1)S(1)} copy(bf16[1,128,4096]{1,2,0:T(8,128)(2,1)S(1)} %bitcast.397) | data formatting | bytes 2097152 | tf_op jit(solution)/shard_map/reshape | solution.py:152
  102.8 22.4 %reduce.11 = bf16[4096,128]{1,0:T(8,128)(2,1)S(1)} reduce(bf16[4096,1,128]{2,1,0:T(2,128)(2,1)S(1)} %bitcast.391, bf16[]{:T(256)} %broadcast.265), dimensions={1}, to_apply=%bitcast.364.reduce_sub_computation | reduce | bytes 2097154
  126.4 6.5 %all-to-all-start.4 = ((bf16[8,2,32768]{2,1,0:T(2,128)(2,1)}), bf16[8,2,32768]{2,1,0:T(2,128)(2,1)S(1)}, u32[]{:S(2)}, u32[]{:S(2)}) async-start(bf16[8,2,32768]{2,1,0:T(2,128)(2,1)} %reshape.406), calls=%async_computation.4 | async-start | bytes 2097152 | tf_op jit(solution)/shard_map/all_to_all | solution.py:200
  135.3 16.7 %copy.539 = bf16[1,128,4096]{1,0,2:T(2,128)(2,1)S(1)} copy(bf16[1,128,4096]{1,2,0:T(8,128)(2,1)S(1)} %bitcast.398) | data formatting | bytes 2097152 | tf_op jit(solution)/shard_map/reshape | solution.py:152
  152.1 23.3 %reduce.10 = bf16[4096,128]{1,0:T(8,128)(2,1)} reduce(bf16[4096,1,128]{2,1,0:T(2,128)(2,1)S(1)} %bitcast.392, bf16[]{:T(256)} %broadcast.265), dimensions={1}, to_apply=%bitcast.365.reduce_sub_computation | reduce | bytes 2097154
  177.7 6.2 %all-to-all-start.2 = ((bf16[8,2,32768]{2,1,0:T(2,128)(2,1)}), bf16[8,2,32768]{2,1,0:T(2,128)(2,1)}, u32[]{:S(2)}, u32[]{:S(2)}) async-start(bf16[8,2,32768]{2,1,0:T(2,128)(2,1)} %reshape.404), calls=%async_computation.2 | async-start | bytes 2097152 | tf_op jit(solution)/shard_map/all_to_all | solution.py:201
  197.8 3.5 reshape.407
  208.8 4.3 reshape.405
  217.7 4.4 fusion.40
  231.3 4.7 fusion.90
  236.0 4.4 fusion.35
  242.7 2.9 fusion.127
  245.7 4.5 multiply_reduce_fusion.1
  252.6 3.5 fusion.209
  260.1 3.5 fusion.210
  265.1 6.4 %fusion.208 = (f32[4,8,128]{2,1,0:T(8,128)S(1)}, f32[4,8,128]{2,1,0:T(8,128)S(1)}, f32[4,8,128,128]{3,2,1,0:T(8,128)}) fusion(f32[4,8,128,128]{3,2,1,0:T(8,128)S(1)} %copy-done.5, f32[4,8,128,128]{3,2,1,0:T(8,128)S(1)} %bitcast.380, f32[4,8,128,128]{3,2,1,0:T(8,128)S(1)} %bitcast.374, f32[4,8,128]{2,1,0:T(8,128)S(1)} %broadcast_add_fusion), kind=kOutput, calls=%fused_computation.322 | convolution fusion | flops 812113920 | bytes 8437760 | tf_op jit(solution)/shard_map/vmap(jvp(ktn,ksn->kts))/dot_general | solution.py:56
  271.4 6.6 %add_add_fusion.1 = f32[4,8,128,128]{3,2,1,0:T(8,128)} fusion(f32[4,8,128,128]{3,2,1,0:T(8,128)S(1)} %copy-done.6, f32[4,8,128,128]{3,2,1,0:T(8,128)S(1)} %get-tuple-element.122, f32[4,8,128,128]{3,2,1,0:T(8,128)S(1)} %bitcast.381, f32[4,8,128,128]{3,2,1,0:T(8,128)S(1)} %copy-done.5, f32[4,8,128]{2,1,0:T(8,128)S(1)} %broadcast_add_fusion, ...), kind=kOutput, calls=%fused_computation.64 | convolution fusion | flops 809500672 | bytes 10534912 | tf_op jit(solution)/shard_map/vmap(transpose(jvp(ktn,ksn->kts)))/dot_general | solution.py:56
  281.4 4.3 add_add_fusion
  289.0 3.0 broadcast_multiply_fusion.4
  292.7 3.2 fusion.33
  295.9 6.0 %copy.372 = bf16[1,1024,512]{2,0,1:T(2,128)(2,1)} copy(bf16[1,1024,512]{1,2,0:T(8,128)(2,1)} %bitcast.413) | data formatting | bytes 2097152 | tf_op jit(solution)/shard_map/reshape | solution.py:261
  301.9 9.0 %reduce.15 = bf16[1024,512]{1,0:T(8,128)(2,1)} reduce(bf16[1024,1,512]{2,1,0:T(2,128)(2,1)} %bitcast.393, bf16[]{:T(256)} %broadcast.265), dimensions={1}, to_apply=%bitcast.308.reduce_sub_computation | reduce | bytes 2097154
  313.5 4.4 all-to-all-start.6
  321.1 5.0 reduce-window.16
  326.4 3.0 broadcast_multiply_fusion.9
  330.0 3.3 fusion.34
  333.3 5.9 %copy.359 = bf16[1,1024,512]{2,0,1:T(2,128)(2,1)} copy(bf16[1,1024,512]{1,2,0:T(8,128)(2,1)} %bitcast.414) | data formatting | bytes 2097152 | tf_op jit(solution)/shard_map/reshape | solution.py:254
  339.3 9.0 %reduce.16 = bf16[1024,512]{1,0:T(8,128)(2,1)} reduce(bf16[1024,1,512]{2,1,0:T(2,128)(2,1)} %bitcast.394, bf16[]{:T(256)} %broadcast.265), dimensions={1}, to_apply=%bitcast.310.reduce_sub_computation | reduce | bytes 2097154
  351.1 4.1 fusion.26
  355.2 6.0 %all-to-all-start.5 = ((bf16[8,2,32768]{2,1,0:T(2,128)(2,1)}), bf16[8,2,32768]{2,1,0:T(2,128)(2,1)}, u32[]{:S(2)}, u32[]{:S(2)}) async-start(bf16[8,2,32768]{2,1,0:T(2,128)(2,1)} %reshape.416), calls=%async_computation.5 | async-start | bytes 2097152 | tf_op jit(solution)/shard_map/all_to_all | solution.py:253
  361.3 5.5 %fusion.41 = f32[4,8,128,64]{2,3,1,0:T(8,128)S(1)} fusion(f32[4,8,128,128]{3,2,1,0:T(8,128)S(1)} %bitcast.376, f32[4,8,128]{2,1,0:T(8,128)S(1)} %get-tuple-element.102, f32[4,8,128,64]{2,1,3,0:T(8,128)} %copy-done.10), kind=kOutput, calls=%fused_computation.71 | convolution fusion | flops 403177472 | bytes 4210688 | tf_op jit(solution)/shard_map/vmap(transpose(jvp(ksn,ksp->knp)))/dot_general | solution.py:64
  366.8 4.2 fusion.57
  378.1 3.8 reduce.17
  382.8 4.3 reshape.415
  388.8 6.0 %all-to-all-start.8 = ((bf16[8,2,256]{2,1,0:T(2,128)(2,1)}), bf16[8,2,256]{2,1,0:T(2,128)(2,1)S(1)}, u32[]{:S(2)}, u32[]{:S(2)}) async-start(bf16[8,2,256]{2,1,0:T(2,128)(2,1)} %reshape.420), calls=%async_computation.8 | async-start | bytes 16384 | tf_op jit(solution)/shard_map/all_to_all | solution.py:267
  394.8 4.3 reshape.417
  400.9 7.3 %all_gather.7 = bf16[512,512]{0,1:T(8,128)(2,1)S(1)} all-gather(bf16[128,512]{0,1:T(8,128)(2,1)S(1)} %pad_maximum_fusion.1), channel_id=1, replica_groups=mesh['sp'=8,'dp'=4] {'dp'}, dimensions={0}, use_global_device_ids=true | all-gather | bytes 655360 | tf_op jit(solution)/shard_map/all_gather | solution.py:289
  408.3 6.0 %all-to-all-start.7 = ((bf16[8,2,16384]{2,1,0:T(2,128)(2,1)}), bf16[8,2,16384]{2,1,0:T(2,128)(2,1)S(1)}, u32[]{:S(2)}, u32[]{:S(2)}) async-start(bf16[8,2,16384]{2,1,0:T(2,128)(2,1)} %reshape.418), calls=%async_computation.7 | async-start | bytes 1048576 | tf_op jit(solution)/shard_map/all_to_all | solution.py:244
  417.4 17.0 %all-to-all-done.7 = bf16[8,2,16384]{2,1,0:T(2,128)(2,1)S(1)} async-done(((bf16[8,2,16384]{2,1,0:T(2,128)(2,1)}), bf16[8,2,16384]{2,1,0:T(2,128)(2,1)S(1)}, u32[]{:S(2)}, u32[]{:S(2)}) %all-to-all-start.7) | async-done | bytes 524320 | tf_op jit(solution)/shard_map/all_to_all | solution.py:244
  439.7 58.7 %all-reduce.26.cloned.1.call-done = f32[512,512]{0,1:T(8,128)} async-done(((f32[512,512]{0,1:T(8,128)}), f32[512,512]{0,1:T(8,128)}) %all-reduce.26.cloned.1.call-update) | async-done | bytes 1048592 | tf_op jit(solution)/shard_map/psum | solution.py:291
  (226 shorter events, 108.4 us)
Async XLA Ops:
  7.2 76.3 %all-gather.2.cloned.1.call-start = ((), (), s32[]{:S(2)}) async-start(), calls=%async_computation.10 | async-start | bytes 2621440 | tf_op jit(solution)/shard_map/all_gather | solution.py:183
  11.6 22.2 %all-to-all-start.1 = ((bf16[8,2,256]{2,1,0:T(2,128)(2,1)}), bf16[8,2,256]{2,1,0:T(2,128)(2,1)S(1)}, u32[]{:S(2)}, u32[]{:S(2)}) async-start(bf16[8,2,256]{2,1,0:T(2,128)(2,1)} %reshape.408), calls=%async_computation.1 | async-start | bytes 16384 | tf_op jit(solution)/shard_map/all_to_all | solution.py:202
  21.3 16.0 %copy-start.28 = (f32[2048]{0:T(1024)S(1)}, f32[2048]{0:T(1024)}, u32[]{:S(2)}) copy-start(f32[2048]{0:T(1024)} %param.31) | copy-start | bytes 24580
  21.3 16.0 %copy-start.27 = (bf16[1,128,2048]{2,1,0:T(8,128)(2,1)S(1)}, bf16[1,128,2048]{2,1,0:T(8,128)(2,1)}, u32[]{:S(2)}) copy-start(bf16[1,128,2048]{2,1,0:T(8,128)(2,1)} %param.19) | copy-start | bytes 1572868
  33.8 17.5 %all-to-all-start.9 = ((bf16[4,2,32768]{2,1,0:T(2,128)(2,1)}), bf16[4,2,32768]{2,1,0:T(2,128)(2,1)S(1)}, u32[]{:S(2)}, u32[]{:S(2)}) async-start(bf16[4,2,32768]{2,1,0:T(2,128)(2,1)} %reshape.422), calls=%async_computation.9 | async-start | bytes 1048576 | tf_op jit(solution)/shard_map/all_to_all | solution.py:287
  37.3 13.3 %copy-start.22 = (bf16[1,128,2048]{2,1,0:T(8,128)(2,1)S(1)}, bf16[1,128,2048]{2,1,0:T(8,128)(2,1)}, u32[]{:S(2)}) copy-start(bf16[1,128,2048]{2,1,0:T(8,128)(2,1)} %param.22) | copy-start | bytes 1572868
  38.1 12.6 %copy-start.21 = (bf16[1,128,2048]{2,1,0:T(8,128)(2,1)S(1)}, bf16[1,128,2048]{2,1,0:T(8,128)(2,1)}, u32[]{:S(2)}) copy-start(bf16[1,128,2048]{2,1,0:T(8,128)(2,1)} %param.21) | copy-start | bytes 1572868
  49.7 1.2 copy-start.20
  51.3 6.8 %copy-start.31 = (f32[5,256]{1,0:T(8,128)S(1)}, f32[5,256]{1,0:T(8,128)}, u32[]{:S(2)}) copy-start(f32[5,256]{1,0:T(8,128)} %param.26) | copy-start | bytes 15364
  51.3 7.0 %copy-start.23 = (bf16[4,2,32768]{2,1,0:T(2,128)(2,1)}, bf16[4,2,32768]{2,1,0:T(2,128)(2,1)S(1)}, u32[]{:S(2)}) copy-start(bf16[4,2,32768]{2,1,0:T(2,128)(2,1)S(1)} %all-to-all-done.9) | copy-start | bytes 1572868
  51.3 25.6 %all-to-all-start = ((bf16[8,2,16384]{2,1,0:T(2,128)(2,1)}), bf16[8,2,16384]{2,1,0:T(2,128)(2,1)}, u32[]{:S(2)}, u32[]{:S(2)}) async-start(bf16[8,2,16384]{2,1,0:T(2,128)(2,1)} %reshape.410), calls=%async_computation | async-start | bytes 1048576 | tf_op jit(solution)/shard_map/all_to_all | solution.py:199
  64.4 19.1 %copy-start.25 = (bf16[1,128,2048]{2,1,0:T(8,128)(2,1)S(1)}, bf16[1,128,2048]{2,1,0:T(8,128)(2,1)}, u32[]{:S(2)}) copy-start(bf16[1,128,2048]{2,1,0:T(8,128)(2,1)} %param.16) | copy-start | bytes 1572868
  76.9 49.5 %all-to-all-start.3 = ((bf16[8,2,16384]{2,1,0:T(2,128)(2,1)}), bf16[8,2,16384]{2,1,0:T(2,128)(2,1)}, u32[]{:S(2)}, u32[]{:S(2)}) async-start(bf16[8,2,16384]{2,1,0:T(2,128)(2,1)} %reshape.412), calls=%async_computation.3 | async-start | bytes 1048576 | tf_op jit(solution)/shard_map/all_to_all | solution.py:203
  125.2 7.7 %copy-start.35 = (f32[4]{0:T(128)S(1)}, f32[4]{0:T(128)}, u32[]{:S(2)}) copy-start(f32[4]{0:T(128)} %param.29) | copy-start | bytes 52
  125.2 7.7 %copy-start.32 = (f32[5,256]{1,0:T(8,128)S(1)}, f32[5,256]{1,0:T(8,128)}, u32[]{:S(2)}) copy-start(f32[5,256]{1,0:T(8,128)} %param.27) | copy-start | bytes 15364
  125.2 7.7 %copy-start.30 = (f32[5,256]{1,0:T(8,128)S(1)}, f32[5,256]{1,0:T(8,128)}, u32[]{:S(2)}) copy-start(f32[5,256]{1,0:T(8,128)} %param.25) | copy-start | bytes 15364
  125.3 8.1 %copy-start.29 = (f32[1,1024,4]{1,2,0:T(4,128)S(1)}, f32[1,1024,4]{1,2,0:T(4,128)}, u32[]{:S(2)}) copy-start(f32[1,1024,4]{1,2,0:T(4,128)} %param.24) | copy-start | bytes 49156
  125.3 8.1 %copy-start.33 = (f32[4]{0:T(128)S(1)}, f32[4]{0:T(128)}, u32[]{:S(2)}) copy-start(f32[4]{0:T(128)} %param.28) | copy-start | bytes 52
  126.4 51.2 %all-to-all-start.4 = ((bf16[8,2,32768]{2,1,0:T(2,128)(2,1)}), bf16[8,2,32768]{2,1,0:T(2,128)(2,1)S(1)}, u32[]{:S(2)}, u32[]{:S(2)}) async-start(bf16[8,2,32768]{2,1,0:T(2,128)(2,1)} %reshape.406), calls=%async_computation.4 | async-start | bytes 2097152 | tf_op jit(solution)/shard_map/all_to_all | solution.py:200
  175.4 9.0 %copy-start.24 = (bf16[4,2,32768]{2,1,0:T(2,128)(2,1)S(1)}, bf16[4,2,32768]{2,1,0:T(2,128)(2,1)}, u32[]{:S(2)}) copy-start(bf16[4,2,32768]{2,1,0:T(2,128)(2,1)} %copy-done.23) | copy-start | bytes 1572868
  177.7 7.4 %copy-start.15 = (bf16[8,2,32768]{2,1,0:T(2,128)(2,1)}, bf16[8,2,32768]{2,1,0:T(2,128)(2,1)S(1)}, u32[]{:S(2)}) copy-start(bf16[8,2,32768]{2,1,0:T(2,128)(2,1)S(1)} %all-to-all-done.4) | copy-start | bytes 3145732
  177.7 31.2 %all-to-all-start.2 = ((bf16[8,2,32768]{2,1,0:T(2,128)(2,1)}), bf16[8,2,32768]{2,1,0:T(2,128)(2,1)}, u32[]{:S(2)}, u32[]{:S(2)}) async-start(bf16[8,2,32768]{2,1,0:T(2,128)(2,1)} %reshape.404), calls=%async_computation.2 | async-start | bytes 2097152 | tf_op jit(solution)/shard_map/all_to_all | solution.py:201
  193.1 4.8 copy-start.2
  195.5 2.4 copy-start.16
  224.2 5.4 %copy-start = (f32[4,1024,128]{2,1,0:T(8,128)}, f32[4,1024,128]{2,1,0:T(8,128)S(1)}, u32[]{:S(2)}) copy-start(f32[4,1024,128]{2,1,0:T(8,128)S(1)} %copy.338) | copy-start | bytes 6291460
  224.3 2.9 copy-start.3
  227.2 4.1 copy-start.7
  231.2 4.8 copy-start.10
  231.3 4.8 copy-start.13
  242.7 3.0 copy-start.6
  245.7 4.5 copy-start.11
  250.4 2.2 copy-start.9
  257.8 2.2 copy-start.8
  260.0 5.0 copy-start.1
  260.0 5.0 copy-start.5
  271.4 6.6 %copy-start.4 = (bf16[1024,4,64]{0,2,1:T(8,128)(2,1)S(1)}, bf16[1024,4,64]{0,2,1:T(8,128)(2,1)}, u32[]{:S(2)}) copy-start(bf16[1024,4,64]{0,2,1:T(8,128)(2,1)} %copy-done.2) | copy-start | bytes 1572868
  313.5 41.7 %all-to-all-start.6 = ((bf16[8,2,32768]{2,1,0:T(2,128)(2,1)}), bf16[8,2,32768]{2,1,0:T(2,128)(2,1)}, u32[]{:S(2)}, u32[]{:S(2)}) async-start(bf16[8,2,32768]{2,1,0:T(2,128)(2,1)} %reshape.414), calls=%async_computation.6 | async-start | bytes 2097152 | tf_op jit(solution)/shard_map/all_to_all | solution.py:260
  355.2 33.5 %all-to-all-start.5 = ((bf16[8,2,32768]{2,1,0:T(2,128)(2,1)}), bf16[8,2,32768]{2,1,0:T(2,128)(2,1)}, u32[]{:S(2)}, u32[]{:S(2)}) async-start(bf16[8,2,32768]{2,1,0:T(2,128)(2,1)} %reshape.416), calls=%async_computation.5 | async-start | bytes 2097152 | tf_op jit(solution)/shard_map/all_to_all | solution.py:253
  361.3 5.5 %copy-start.12 = (f32[4,8,128,64]{2,1,3,0:T(8,128)S(1)}, f32[4,8,128,64]{2,1,3,0:T(8,128)}, u32[]{:S(2)}) copy-start(f32[4,8,128,64]{2,1,3,0:T(8,128)} %copy-done.11) | copy-start | bytes 3145732
  361.3 5.5 %copy-start.17 = (f32[4,8,128,64]{2,3,1,0:T(8,128)S(1)}, f32[4,8,128,64]{2,3,1,0:T(8,128)}, u32[]{:S(2)}) copy-start(f32[4,8,128,64]{2,3,1,0:T(8,128)} %fusion.26) | copy-start | bytes 3145732
  366.8 4.2 copy-start.19
  366.8 4.2 copy-start.34
  388.8 19.5 %all-to-all-start.8 = ((bf16[8,2,256]{2,1,0:T(2,128)(2,1)}), bf16[8,2,256]{2,1,0:T(2,128)(2,1)S(1)}, u32[]{:S(2)}, u32[]{:S(2)}) async-start(bf16[8,2,256]{2,1,0:T(2,128)(2,1)} %reshape.420), calls=%async_computation.8 | async-start | bytes 16384 | tf_op jit(solution)/shard_map/all_to_all | solution.py:267
  399.4 1.2 copy-start.18
  400.6 13.7 %copy-start.26 = (bf16[4,1,128,512]{3,2,0,1:T(8,128)(2,1)S(1)}, bf16[4,1,128,512]{3,2,0,1:T(8,128)(2,1)}, u32[]{:S(2)}) copy-start(bf16[4,1,128,512]{3,2,0,1:T(8,128)(2,1)} %copy.390) | copy-start | bytes 1572868
  408.3 26.1 %all-to-all-start.7 = ((bf16[8,2,16384]{2,1,0:T(2,128)(2,1)}), bf16[8,2,16384]{2,1,0:T(2,128)(2,1)S(1)}, u32[]{:S(2)}, u32[]{:S(2)}) async-start(bf16[8,2,16384]{2,1,0:T(2,128)(2,1)} %reshape.418), calls=%async_computation.7 | async-start | bytes 1048576 | tf_op jit(solution)/shard_map/all_to_all | solution.py:244
  414.3 84.2 %all-reduce.26.cloned.1.call-start = ((), (), s32[]{:S(2)}) async-start(), calls=%async_computation.11 | async-start | bytes 2097152 | tf_op jit(solution)/shard_map/psum | solution.py:291
  434.9 3.2 copy-start.14
Sparse Core Ops, SparseCore 0:
  10.1 25.2 all-gather.1
  418.6 79.7 all-reduce.25
where the time goes:
time: 519 us; the launch traced here: 509 us
  other arithmetic  148 us (29%)
  local copies, waits for them, and re-layouts  125 us (24%)
  waiting for transfers between devices  78.6 us (15%)
  matrix products  76 us (15%)
  starting transfers between devices  58.5 us (11%)
  between operations  15.7 us (3%)
  blocking collectives  7.34 us (1%)
    unnamed x15, other arithmetic  108 us
    psum x1, waiting for transfers between devices, local(): total_grad = lax.psum(local_rows, 'sp')  58.7 us
    unnamed x111, local copies, waits for them, and re-layouts  46.7 us
    reshape x2, local copies, waits for them, and re-layouts, spread_heads(): return copied.reshape(1, tokens, HEADS * STATE)  33.5 us
    dot_general x3, matrix products, one_channel_scan(): jnp.einsum('ktn,ksn->kts', reading, keyed, precision=highest) * within  17.2 us
    all_to_all x1, waiting for transfers between devices, local(): lax.all_to_all(jnp.transpose(source_derivative, (1, 0, 2)).reshape(1, win...  17 us
    another operation x8, other arithmetic  14.2 us
    dot_general x3, matrix products, one_channel_scan(): jnp.einsum('ksn,ksp->knp', keyed * weight_fwd[:, :, None], driven, precis...  12.4 us
  transfers between devices with their start and end apart: 12, of which 3 were waited for; matrix products, arithmetic and copies ran while one was open for 47% of the time, Pallas kernels for 0%

commit v1 on v0

v1 whole, which is shorter than its diff:
```python
import functools

import jax
import jax.numpy as jnp
from jax import lax
from jax.experimental import pallas as pl
from jax.experimental.pallas import tpu as pltpu
from jax.sharding import PartitionSpec as P

HEADS = 32
HEAD_DIM = 64
STATE = 128
GROUPS = 2
NORM_GROUPS = 8
CONV_K = 5
BLOCK = 128
INNER = 2048
LANES = 128
HALO = 8
EPSILON = 1e-06
LOG2E = 1.4426950408889634
highest = lax.Precision.HIGHEST
f32 = jnp.float32
bf16 = jnp.bfloat16


def sigmoid(v):
    return 1.0 / (1.0 + jnp.exp(-v))


def softplus(v):
    e = jnp.exp(-jnp.abs(v))
    z = e / (2.0 + e)
    z2 = z * z
    series = jnp.full_like(z, 1.0 / 17.0)
    for odd in (15, 13, 11, 9, 7, 5, 3, 1):
        series = series * z2 + 1.0 / odd
    return jnp.maximum(v, 0.0) + 2.0 * z * series


def norm_kernel(values_ref, gates_ref, adjoint_ref, scale_ref, dy_ref, dgate_ref):
    values = values_ref[...].astype(f32)
    gates = gates_ref[...].astype(f32)
    sig = sigmoid(gates)
    act = gates * sig
    g = values * act
    dn = adjoint_ref[...].astype(f32) * scale_ref[...]
    width = g.shape[1]
    inv = lax.rsqrt(jnp.sum(g * g, axis=1, keepdims=True) * (1.0 / width) + EPSILON)
    along = jnp.sum(dn * g, axis=1, keepdims=True) * (1.0 / width)
    dg = inv * dn - g * (inv * inv * inv * along)
    dy_ref[...] = (dg * act).astype(bf16)
    dgate_ref[...] = (dg * values * (sig + act * (1.0 - sig))).astype(bf16)


def norm_backward(values, gates, adjoint, scale):
    tokens, inner = values.shape
    width = inner // NORM_GROUPS
    block = pl.BlockSpec((tokens, width), lambda i: (0, i))
    return pl.pallas_call(
        norm_kernel,
        grid=(NORM_GROUPS,),
        in_specs=[block, block, block, pl.BlockSpec((1, width), lambda i: (0, i))],
        out_specs=[block, block],
        out_shape=[jax.ShapeDtypeStruct((tokens, inner), bf16)] * 2,
        name="norm_backward",
    )(values, gates, adjoint, scale.reshape(1, inner))


def window_conv(padded, r0, taps, flip):
    rows = padded[pl.ds(r0, BLOCK + 2 * HALO), :]
    total = None
    for k in range(CONV_K):
        shift = HALO - CONV_K // 2 + k
        tap = taps[CONV_K - 1 - k if flip else k][None, :]
        term = tap * pltpu.roll(rows, rows.shape[0] - shift, axis=0)[:BLOCK]
        total = term if total is None else total + term
    return total


def mixer_kernel(
    heads,
    tile,
    p1_ref,
    p2_ref,
    drop_ref,
    tapx_ref,
    tapbc_ref,
    par_ref,
    out_ref,
    pad_x,
    pad_bc,
    u_ref,
    sux_ref,
    sbc_ref,
    dtc_ref,
    sig_ref,
    lcol,
    lrow,
    kt,
    rt,
    kn,
    rn,
    vt,
    dyt,
    dyh,
    dvt,
    dkt,
    dr,
    rowacc,
    rowdl,
    colsum,
):
    window = p1_ref.shape[0]
    xw = u_ref.shape[1]
    chunks = window // BLOCK
    tapx = tapx_ref[...]
    tapbc = tapbc_ref[...]
    offset = par_ref[0:1, :]
    fade = par_ref[1:2, :]
    skip = tapx[CONV_K : CONV_K + 1]
    lane_head = lax.broadcasted_iota(jnp.int32, (BLOCK, xw), 1) // HEAD_DIM
    row_i = lax.broadcasted_iota(jnp.int32, (BLOCK, BLOCK), 0)
    col_i = lax.broadcasted_iota(jnp.int32, (BLOCK, BLOCK), 1)
    lower = (row_i >= col_i).astype(f32)
    upper = (row_i <= col_i).astype(f32)

    def spread(columns):
        out = jnp.zeros((BLOCK, xw), f32)
        for h in range(heads):
            out = jnp.where(lane_head == h, columns[:, h : h + 1], out)
        return out

    for padded in (pad_x, pad_bc):
        padded[0:HALO, :] = jnp.zeros((HALO, padded.shape[1]), f32)
        padded[HALO + window :, :] = jnp.zeros((HALO, padded.shape[1]), f32)

    @pl.loop(0, chunks)
    def _(c):
        r0 = pl.multiple_of(c * BLOCK, BLOCK)
        rows = pl.ds(r0, BLOCK)
        into = pl.ds(pl.multiple_of(r0 + HALO, HALO), BLOCK)
        pad_x[into, :] = p1_ref[rows, :xw].astype(f32)
        pad_bc[into, :] = p2_ref[rows, xw:].astype(f32)

    def prepare(c, carry):
        r0 = pl.multiple_of(c * BLOCK, BLOCK)
        rows = pl.ds(r0, BLOCK)
        a = p1_ref[rows, xw:].astype(f32) + offset
        dt = softplus(a)
        dtc_ref[rows, :] = dt
        sig_ref[rows, :] = sigmoid(a)
        rate = dt * fade + drop_ref[rows, :]
        level = jnp.dot(lower, rate, precision=highest, preferred_element_type=f32) + carry
        scaled = level * LOG2E
        lcol[rows, :] = scaled
        lrow[:, rows] = scaled.T[: lrow.shape[0]]
        pre = window_conv(pad_x, r0, tapx, False)
        sig = sigmoid(pre)
        u = pre * sig
        u_ref[rows, :] = u
        sux_ref[rows, :] = sig + u * (1.0 - sig)
        vt[:, rows] = (u * spread(dt)).T.astype(bf16)
        dy_t = p2_ref[rows, :xw].astype(f32).T
        dyt[:, rows] = dy_t.astype(bf16)
        for h in range(heads):
            dyh[h, rows, :] = dy_t[h * HEAD_DIM : (h + 1) * HEAD_DIM].T.astype(bf16)
        pre = window_conv(pad_bc, r0, tapbc, False)
        sig = sigmoid(pre)
        kr = pre * sig
        sbc_ref[rows, :] = sig + kr * (1.0 - sig)
        kn[rows, :] = kr[:, :STATE].astype(bf16)
        rn[rows, :] = kr[:, STATE:].astype(bf16)
        kt[:, rows] = kr[:, :STATE].T.astype(bf16)
        rt[:, rows] = kr[:, STATE:].T.astype(bf16)
        return level[BLOCK - 1 : BLOCK]

    lax.fori_loop(0, chunks, prepare, jnp.zeros((1, LANES), f32))

    dvt[...] = jnp.zeros_like(dvt)
    dkt[...] = jnp.zeros_like(dkt)
    colsum[...] = jnp.zeros_like(colsum)
    rowdl[...] = jnp.zeros_like(rowdl)
    ahead = lax.broadcasted_iota(jnp.int32, (tile, tile), 0) - lax.broadcasted_iota(
        jnp.int32, (tile, tile), 1
    )

    @pl.loop(0, window // tile)
    def _(ti):
        t0 = pl.multiple_of(ti * tile, tile)
        ts = pl.ds(t0, tile)
        rowacc[...] = jnp.zeros_like(rowacc)
        dr[ts, :] = jnp.zeros((tile, STATE), f32)
        reads = rn[ts, :]
        reads_t = rt[:, ts]

        @pl.loop(0, window // tile)
        def _(si):
            s0 = pl.multiple_of(si * tile, tile)
            ss = pl.ds(s0, tile)
            score = jnp.dot(reads, kt[:, ss], preferred_element_type=f32)
            order = jnp.clip(ahead + (t0 - s0), -1, 1).astype(f32)
            signed = score * order
            ge_sum = None
            for h in range(heads):
                hs = slice(h * HEAD_DIM, (h + 1) * HEAD_DIM)
                gap = lcol[ts, h : h + 1] - lrow[h : h + 1, ss]
                decay = jnp.exp2(-jnp.abs(gap))
                g = jnp.dot(dyh[h, ts, :], vt[hs, ss], preferred_element_type=f32)
                ge = g * decay
                ge_sum = ge if ge_sum is None else ge_sum + ge
                se = (score * decay).astype(bf16)
                dvt[hs, ss] += jnp.dot(dyt[hs, ts], se, preferred_element_type=f32)
                pair = signed * ge
                colsum[h : h + 1, ss] += jnp.sum(pair, axis=0, keepdims=True)
                part = pair[:, :LANES]
                for piece in range(1, tile // LANES):
                    part = part + pair[:, piece * LANES : (piece + 1) * LANES]
                rowacc[h] += part
            ge_b = ge_sum.astype(bf16)
            dr[ts, :] += jnp.dot(ge_b, kn[ss, :], preferred_element_type=f32)
            dkt[:, ss] += jnp.dot(reads_t, ge_b, preferred_element_type=f32)

        for h in range(heads):
            rowdl[ts, h : h + 1] = -jnp.sum(rowacc[h], axis=1, keepdims=True)

    def finish(i, carry):
        r0 = pl.multiple_of((chunks - 1 - i) * BLOCK, BLOCK)
        rows = pl.ds(r0, BLOCK)
        into = pl.ds(pl.multiple_of(r0 + HALO, HALO), BLOCK)
        dlevel = rowdl[rows, :] + colsum[:, rows].T
        drate = jnp.dot(upper, dlevel, precision=highest, preferred_element_type=f32) + carry
        dv = dvt[:, rows].T
        u = u_ref[rows, :]
        udv = u * dv
        lane = lax.broadcasted_iota(jnp.int32, (BLOCK, LANES), 1)
        ddt = drate * fade
        for h in range(heads):
            along = jnp.sum(jnp.where(lane_head == h, udv, 0.0), axis=1, keepdims=True)
            ddt = ddt + jnp.where(lane == h, along, 0.0)
        out_ref[rows, xw + 2 * STATE :] = (ddt * sig_ref[rows, :]).astype(bf16)
        du = dv * spread(dtc_ref[rows, :]) + skip * p2_ref[rows, :xw].astype(f32)
        pad_x[into, :] = du * sux_ref[rows, :]
        sbc = sbc_ref[rows, :]
        pad_bc[into, :STATE] = dkt[:, rows].T * sbc[:, :STATE]
        pad_bc[into, STATE:] = dr[rows, :] * sbc[:, STATE:]
        return carry + jnp.sum(dlevel, axis=0, keepdims=True)

    lax.fori_loop(0, chunks, finish, jnp.zeros((1, LANES), f32))

    @pl.loop(0, chunks)
    def _(c):
        r0 = pl.multiple_of(c * BLOCK, BLOCK)
        rows = pl.ds(r0, BLOCK)
        out_ref[rows, :xw] = window_conv(pad_x, r0, tapx, True).astype(bf16)
        out_ref[rows, xw : xw + 2 * STATE] = window_conv(pad_bc, r0, tapbc, True).astype(bf16)


def mixer_backward(p1, p2, drop, tapx, tapbc, par, heads):
    window = p1.shape[0]
    xw = tapx.shape[1]
    tile = 2 * BLOCK if window % (2 * BLOCK) == 0 else BLOCK
    rows_h = -(-heads // 8) * 8
    scratch = [
        pltpu.VMEM((window + 2 * HALO, xw), f32),
        pltpu.VMEM((window + 2 * HALO, 2 * STATE), f32),
        pltpu.VMEM((window, xw), f32),
        pltpu.VMEM((window, xw), f32),
        pltpu.VMEM((window, 2 * STATE), f32),
        pltpu.VMEM((window, LANES), f32),
        pltpu.VMEM((window, LANES), f32),
        pltpu.VMEM((window, LANES), f32),
        pltpu.VMEM((rows_h, window), f32),
        pltpu.VMEM((STATE, window), bf16),
        pltpu.VMEM((STATE, window), bf16),
        pltpu.VMEM((window, STATE), bf16),
        pltpu.VMEM((window, STATE), bf16),
        pltpu.VMEM((xw, window), bf16),
        pltpu.VMEM((xw, window), bf16),
        pltpu.VMEM((heads, window, HEAD_DIM), bf16),
        pltpu.VMEM((xw, window), f32),
        pltpu.VMEM((STATE, window), f32),
        pltpu.VMEM((window, STATE), f32),
        pltpu.VMEM((heads, tile, LANES), f32),
        pltpu.VMEM((window, LANES), f32),
        pltpu.VMEM((LANES, window), f32),
    ]
    return pl.pallas_call(
        functools.partial(mixer_kernel, heads, tile),
        in_specs=[pl.BlockSpec(memory_space=pltpu.VMEM)] * 6,
        out_specs=pl.BlockSpec(memory_space=pltpu.VMEM),
        out_shape=jax.ShapeDtypeStruct((window, xw + 2 * STATE + LANES), bf16),
        scratch_shapes=scratch,
        compiler_params=pltpu.CompilerParams(vmem_limit_bytes=62 * 1024 * 1024),
        name="mixer_backward",
    )(p1, p2, drop, tapx, tapbc, par)


def pad_last(values, width):
    pads = [(0, 0)] * (values.ndim - 1) + [(0, width - values.shape[-1])]
    return jnp.pad(values, pads)


def exchange(values, axis):
    return lax.all_to_all(values, axis, split_axis=0, concat_axis=0, tiled=True)


def by_owner(values, owners):
    tokens, width = values.shape
    return jnp.transpose(values.reshape(tokens, owners, width // owners), (1, 0, 2))


def local(
    layer_activity,
    writer_matrix,
    reader_matrix,
    source_unfiltered,
    switch_raw_signal,
    saved_result,
    final_adjoint,
    delta_raw,
    extra_logdrop,
    source_filter_coefs,
    writer_filter_coefs,
    reader_filter_coefs,
    delta_offset,
    fading_exponents,
    direct_factor,
    rescale_factor,
):
    tokens = layer_activity.shape[1]
    width_in = layer_activity.shape[2]
    latent = GROUPS * STATE
    dp = lax.axis_size("dp")
    sp = lax.axis_size("sp")
    heads = delta_offset.shape[0]
    per_group = HEADS // GROUPS
    xc = heads * HEAD_DIM
    xw = -(-xc // LANES) * LANES
    window = tokens * sp

    columns = exchange(by_owner(layer_activity.reshape(tokens, width_in), dp), "dp")
    columns = columns.reshape(dp * tokens, width_in // dp)
    weights = jnp.concatenate([writer_matrix, reader_matrix], axis=1)
    partial = jnp.dot(columns, weights, preferred_element_type=f32).astype(bf16)
    p1 = exchange(
        jnp.concatenate(
            [
                pad_last(by_owner(source_unfiltered.reshape(tokens, INNER), sp), xw),
                pad_last(by_owner(delta_raw.reshape(tokens, HEADS), sp), LANES),
            ],
            axis=2,
        ),
        "sp",
    )
    result_adjoint, d_gate = norm_backward(
        saved_result.reshape(tokens, INNER),
        switch_raw_signal.reshape(tokens, INNER),
        final_adjoint.reshape(tokens, INNER),
        rescale_factor,
    )
    partial = exchange(partial.reshape(dp, tokens, 2 * latent), "dp")
    projected = jnp.sum(partial.astype(f32), axis=0).astype(bf16)
    maps = jnp.transpose(projected.reshape(tokens, 2, GROUPS, STATE), (2, 0, 1, 3))
    maps = jnp.broadcast_to(
        maps.reshape(GROUPS, 1, tokens, 2 * STATE), (GROUPS, sp // GROUPS, tokens, 2 * STATE)
    ).reshape(sp, tokens, 2 * STATE)
    p2 = exchange(
        jnp.concatenate([pad_last(by_owner(result_adjoint, sp), xw), maps], axis=2), "sp"
    )

    group = lax.axis_index("sp") * heads // per_group
    tapbc = jnp.concatenate(
        [
            lax.dynamic_slice_in_dim(writer_filter_coefs, group * STATE, STATE, axis=1),
            lax.dynamic_slice_in_dim(reader_filter_coefs, group * STATE, STATE, axis=1),
        ],
        axis=1,
    )
    par = pad_last(jnp.stack([delta_offset, jnp.exp(fading_exponents)]), LANES)
    back = mixer_backward(
        p1.reshape(window, xw + LANES),
        p2.reshape(window, xw + 2 * STATE),
        pad_last(extra_logdrop.reshape(window, heads), LANES),
        pad_last(
            jnp.concatenate([source_filter_coefs, jnp.repeat(direct_factor, HEAD_DIM)[None]]), xw
        ),
        tapbc,
        par,
        heads,
    )
    back = exchange(back.reshape(sp, tokens, xw + 2 * STATE + LANES), "sp")
    back_x = jnp.transpose(back[:, :, :xc], (1, 0, 2)).reshape(1, tokens, INNER)
    back_dt = jnp.transpose(
        back[:, :, xw + 2 * STATE : xw + 2 * STATE + heads], (1, 0, 2)
    ).reshape(1, tokens, HEADS)
    summed = jnp.sum(
        back[:, :, xw : xw + 2 * STATE]
        .astype(f32)
        .reshape(GROUPS, sp // GROUPS, tokens, 2, STATE),
        axis=1,
    )
    gradients = jnp.transpose(summed, (1, 2, 0, 3)).reshape(tokens, 2 * latent).astype(bf16)
    all_grads = exchange(
        jnp.broadcast_to(gradients[None], (dp, tokens, 2 * latent)), "dp"
    ).reshape(dp * tokens, 2 * latent)
    rows = width_in // dp
    local_rows = jnp.einsum("td,tc->dc", columns, all_grads, preferred_element_type=f32)
    shares = exchange(local_rows.astype(bf16).reshape(sp, rows // sp, 2 * latent), "sp")
    share = jnp.sum(shares.astype(f32), axis=0).astype(bf16)
    total_grad = exchange(
        jnp.broadcast_to(share[None], (sp, rows // sp, 2 * latent)), "sp"
    ).reshape(rows, 2 * latent)
    d_cols = jnp.einsum("tc,dc->td", all_grads, weights, preferred_element_type=f32)
    d_hidden = exchange(d_cols.astype(bf16).reshape(dp, tokens, rows), "dp")
    d_hidden = jnp.transpose(d_hidden, (1, 0, 2)).reshape(1, tokens, width_in)
    return (
        d_hidden,
        back_x,
        d_gate.reshape(1, tokens, INNER),
        back_dt,
        total_grad[:, :latent].astype(f32),
        total_grad[:, latent:].astype(f32),
    )


def solution(mesh):
    in_specs = (
        P("dp", "sp", None),
        P("dp", None),
        P("dp", None),
        P("dp", "sp", None),
        P("dp", "sp", None),
        P("dp", "sp", None),
        P("dp", "sp", None),
        P("dp", "sp", None),
        P("dp", None, "sp"),
        P(None, "sp"),
        P(),
        P(),
        P("sp"),
        P("sp"),
        P("sp"),
        P(),
    )
    out_specs = (
        P("dp", "sp", None),
        P("dp", "sp", None),
        P("dp", "sp", None),
        P("dp", "sp", None),
        P("dp", None),
        P("dp", None),
    )
    return jax.shard_map(local, mesh=mesh, in_specs=in_specs, out_specs=out_specs, check_vma=False)
```

time: 519 us -> 213 us (0.41); the launches traced: 509 us -> 212 us
  other arithmetic: 148 us -> 5.76 us
  local copies, waits for them, and re-layouts: 125 us -> 12.2 us
  matrix products: 76 us -> 3.73 us
  blocking collectives: 7.34 us -> 46.4 us
  Pallas kernels: 0 us -> 31.4 us
  starting transfers between devices: 58.5 us -> 28.5 us
  between operations: 15.7 us -> 0.97 us
    unnamed x15 -> x0, other arithmetic: 108 us -> none
    dot_general x26 -> x3, matrix products: 76 us -> 3.73 us  [the longest x1 1.27 us: local(): jnp.einsum('tc,dc->td', all_grads, weights, preferred_element_type=f32)]
    all_to_all x10 -> x7, waiting for transfers between devices: 19.9 us -> 82.6 us  [exchange(): return lax.all_to_all(values, axis, split_axis=0, concat_axis=0, tiled=True)]
    psum x1 -> x0, waiting for transfers between devices: 58.7 us -> none  [local(): total_grad = lax.psum(local_rows, 'sp')]
    reshape x12 -> x4, local copies, waits for them, and re-layouts: 53.1 us -> 3.4 us  [the longest x1 1.17 us: local(): d_hidden = jnp.transpose(d_hidden, (1, 0, 2)).reshape(1, tokens, width_in)]
    all_to_all x0 -> x2, blocking collectives: none -> 46.4 us  [exchange(): return lax.all_to_all(values, axis, split_axis=0, concat_axis=0, tiled=True)]
    unnamed x111 -> x36, local copies, waits for them, and re-layouts: 46.7 us -> 3.49 us
    pallas_call x0 -> x2, Pallas kernels: none -> 31.4 us  [the longest x1 25.6 us: mixer_backward(): pl.pallas_call(functools.partial(mixer_kernel, heads, tile), in_specs=[pl...]
  transfers between devices with their start and end apart: 12 -> 7, of which waited for: 3 -> 7; matrix products, arithmetic and copies ran while one was open for 47% -> 6% of each run, Pallas kernels for 0% -> 3%
where the time goes in v1:
time: 213 us; the launch traced here: 212 us
  waiting for transfers between devices  82.6 us (39%)
  blocking collectives  46.4 us (22%)
  Pallas kernels  31.4 us (15%)
  starting transfers between devices  28.5 us (13%)
  local copies, waits for them, and re-layouts  12.2 us (6%)
  other arithmetic  5.76 us (3%)
  matrix products  3.73 us (2%)
    all_to_all x7, waiting for transfers between devices, exchange(): return lax.all_to_all(values, axis, split_axis=0, concat_axis=0, tiled=True)  82.6 us
    all_to_all x2, blocking collectives, exchange(): return lax.all_to_all(values, axis, split_axis=0, concat_axis=0, tiled=True)  46.4 us
    all_to_all x7, starting transfers between devices, exchange(): return lax.all_to_all(values, axis, split_axis=0, concat_axis=0, tiled=True)  28.5 us
    pallas_call x1, Pallas kernels, mixer_backward(): pl.pallas_call(functools.partial(mixer_kernel, heads, tile), in_specs=[pl...  25.6 us
    pallas_call x1, Pallas kernels, norm_backward(): pl.pallas_call(norm_kernel, grid=(NORM_GROUPS,), in_specs=[block, block,...  5.82 us
  transfers between devices with their start and end apart: 7, of which 7 were waited for; matrix products, arithmetic and copies ran while one was open for 6% of the time, Pallas kernels for 3%

profile of v1, /device:TPU:0, one launch (start us, length us, event | category | flops | bytes accessed | tf_op | source)
XLA Modules:
  0.0 211.5 jit_solution(4933358672667281207)
XLA Ops:
  0.7 2.1 copy.65
  2.7 4.3 %all-to-all-start.1 = ((bf16[4,128,512]{1,2,0:T(8,128)(2,1)}), bf16[4,128,512]{1,2,0:T(8,128)(2,1)S(1)}, u32[]{:S(2)}, u32[]{:S(2)}) async-start(bf16[4,128,512]{1,2,0:T(8,128)(2,1)} %bitcast.10), calls=%async_computation.1 | async-start | bytes 1048576 | tf_op jit(solution)/shard_map/all_to_all | solution.py:305
  7.1 8.7 %all-to-all-done.1 = bf16[4,128,512]{1,2,0:T(8,128)(2,1)S(1)} async-done(((bf16[4,128,512]{1,2,0:T(8,128)(2,1)}), bf16[4,128,512]{1,2,0:T(8,128)(2,1)S(1)}, u32[]{:S(2)}, u32[]{:S(2)}) %all-to-all-start.1) | async-done | bytes 524320 | tf_op jit(solution)/shard_map/all_to_all | solution.py:305
  15.8 0.2 copy.66
  16.1 1.2 convolution_convert_fusion
  17.3 3.5 %all-to-all-start.2 = ((bf16[4,128,512]{2,1,0:T(8,128)(2,1)}), bf16[4,128,512]{2,1,0:T(8,128)(2,1)S(1)}, u32[]{:S(2)}, u32[]{:S(2)}) async-start(bf16[4,128,512]{2,1,0:T(8,128)(2,1)} %bitcast.13), calls=%async_computation.2 | async-start | bytes 1048576 | tf_op jit(solution)/shard_map/all_to_all | solution.py:305
  20.8 0.2 copy.63
  21.0 0.1 copy.77
  21.2 1.0 fusion.2
  22.3 7.3 %all-to-all-done.2 = bf16[4,128,512]{2,1,0:T(8,128)(2,1)S(1)} async-done(((bf16[4,128,512]{2,1,0:T(8,128)(2,1)}), bf16[4,128,512]{2,1,0:T(8,128)(2,1)S(1)}, u32[]{:S(2)}, u32[]{:S(2)}) %all-to-all-start.2) | async-done | bytes 524320 | tf_op jit(solution)/shard_map/all_to_all | solution.py:305
  29.6 6.5 %all-to-all-start = ((bf16[8,128,384]{2,1,0:T(8,128)(2,1)}), bf16[8,128,384]{2,1,0:T(8,128)(2,1)S(1)}, u32[]{:S(2)}, u32[]{:S(2)}) async-start(bf16[8,128,384]{2,1,0:T(8,128)(2,1)} %fusion.2), calls=%async_computation | async-start | bytes 1572864 | tf_op jit(solution)/shard_map/all_to_all | solution.py:305
  36.0 5.8 %norm_backward.1 = (bf16[128,2048]{1,0:T(8,128)(2,1)}, bf16[128,2048]{1,0:T(8,128)(2,1)}) custom-call(bf16[128,2048]{1,0:T(8,128)(2,1)} %bitcast.76, bf16[128,2048]{1,0:T(8,128)(2,1)} %bitcast.77, bf16[128,2048]{1,0:T(8,128)(2,1)} %bitcast.78, f32[1,2048]{1,0:T(1,128)} %bitcast.85), custom_call_target="tpu_custom_call" | custom-call | tf_op jit(solution)/shard_map/norm_backward/pallas_call | solution.py:60
  41.8 1.1 copy.80
  43.0 0.1 copy.67
  43.2 0.1 copy.69
  43.3 1.1 pad_maximum_fusion
  44.4 11.6 %all-to-all-done = bf16[8,128,384]{2,1,0:T(8,128)(2,1)S(1)} async-done(((bf16[8,128,384]{2,1,0:T(8,128)(2,1)}), bf16[8,128,384]{2,1,0:T(8,128)(2,1)S(1)}, u32[]{:S(2)}, u32[]{:S(2)}) %all-to-all-start) | async-done | bytes 786464 | tf_op jit(solution)/shard_map/all_to_all | solution.py:305
  56.0 3.6 %all-to-all-start.3 = ((bf16[8,128,512]{2,1,0:T(8,128)(2,1)}), bf16[8,128,512]{2,1,0:T(8,128)(2,1)S(1)}, u32[]{:S(2)}, u32[]{:S(2)}) async-start(bf16[8,128,512]{2,1,0:T(8,128)(2,1)} %pad_maximum_fusion), calls=%async_computation.3 | async-start | bytes 2097152 | tf_op jit(solution)/shard_map/all_to_all | solution.py:305
  59.8 0.2 copy.70
  60.0 0.8 pad.13.drop_ref
  60.9 0.6 select_maximum_fusion.par_ref
  61.5 0.6 pad_maximum_fusion.1.tapx_ref
  62.1 0.6 pad_maximum_fusion.2.tapbc_ref
  62.7 22.8 %all-to-all-done.3 = bf16[8,128,512]{2,1,0:T(8,128)(2,1)S(1)} async-done(((bf16[8,128,512]{2,1,0:T(8,128)(2,1)}), bf16[8,128,512]{2,1,0:T(8,128)(2,1)S(1)}, u32[]{:S(2)}, u32[]{:S(2)}) %all-to-all-start.3) | async-done | bytes 1048608 | tf_op jit(solution)/shard_map/all_to_all | solution.py:305
  85.4 1.0 copy-done
  86.4 25.6 %mixer_backward.1 = bf16[1024,640]{1,0:T(8,128)(2,1)} custom-call(bf16[1024,384]{1,0:T(8,128)(2,1)} %bitcast.66, bf16[1024,512]{1,0:T(8,128)(2,1)} %bitcast.65, f32[1024,128]{1,0:T(8,128)} %pad.13.drop_ref, f32[6,256]{1,0:T(8,128)} %pad_maximum_fusion.1.tapx_ref, f32[5,256]{1,0:T(8,128)} %pad_maximum_fusion.2.tapbc_ref, f32[2,128]{1,0:T(2,128)} %select_maximum_fusion.par_ref), custom_call_target="tpu_custom_call" | custom-call | tf_op jit(solution)/shard_map/mixer_backward/pallas_call | solution.py:288
  112.0 35.2 %all_to_all.45 = bf16[8,128,640]{2,1,0:T(8,128)(2,1)S(1)} all-to-all(bf16[8,128,640]{2,1,0:T(8,128)(2,1)} %bitcast.63), channel_id=1, replica_groups=mesh['sp'=8,'dp'=4] {'sp'}, dimensions={0} | all-to-all | bytes 2621440 | tf_op jit(solution)/shard_map/all_to_all | solution.py:305
  147.1 0.9 slice_bitcast_fusion
  148.0 0.1 reshape.104
  148.2 0.7 reduce.2
  148.9 0.1 copy.71
  149.0 0.1 copy.72
  149.2 11.2 %all_to_all.46 = bf16[4,128,512]{2,1,0:T(8,128)(2,1)S(1)} all-to-all(bf16[4,128,512]{2,1,0:T(8,128)(2,1)S(1)} %broadcast_in_dim.25), channel_id=1, replica_groups=mesh['sp'=8,'dp'=4] {'dp'}, dimensions={0} | all-to-all | bytes 1048576 | tf_op jit(solution)/shard_map/all_to_all | solution.py:305
  160.4 1.2 fusion.1
  161.6 3.6 %all-to-all-start.7 = ((bf16[8,64,512]{2,1,0:T(8,128)(2,1)}), bf16[8,64,512]{2,1,0:T(8,128)(2,1)S(1)}, u32[]{:S(2)}, u32[]{:S(2)}) async-start(bf16[8,64,512]{2,1,0:T(8,128)(2,1)} %bitcast.34), calls=%async_computation.7 | async-start | bytes 1048576 | tf_op jit(solution)/shard_map/all_to_all | solution.py:305
  165.3 1.3 convolution_convert_fusion.1
  166.5 13.0 %all-to-all-done.7 = bf16[8,64,512]{2,1,0:T(8,128)(2,1)S(1)} async-done(((bf16[8,64,512]{2,1,0:T(8,128)(2,1)}), bf16[8,64,512]{2,1,0:T(8,128)(2,1)S(1)}, u32[]{:S(2)}, u32[]{:S(2)}) %all-to-all-start.7) | async-done | bytes 524320 | tf_op jit(solution)/shard_map/all_to_all | solution.py:305
  179.5 3.5 %all-to-all-start.6 = ((bf16[4,128,512]{2,1,0:T(8,128)(2,1)}), bf16[4,128,512]{2,1,0:T(8,128)(2,1)S(1)}, u32[]{:S(2)}, u32[]{:S(2)}) async-start(bf16[4,128,512]{2,1,0:T(8,128)(2,1)} %bitcast.26), calls=%async_computation.6 | async-start | bytes 1048576 | tf_op jit(solution)/shard_map/all_to_all | solution.py:305
  183.1 8.7 %all-to-all-done.6 = bf16[4,128,512]{2,1,0:T(8,128)(2,1)S(1)} async-done(((bf16[4,128,512]{2,1,0:T(8,128)(2,1)}), bf16[4,128,512]{2,1,0:T(8,128)(2,1)S(1)}, u32[]{:S(2)}, u32[]{:S(2)}) %all-to-all-start.6) | async-done | bytes 524320 | tf_op jit(solution)/shard_map/all_to_all | solution.py:305
  191.7 0.8 broadcast_in_dim.26
  192.6 3.6 %all-to-all-start.8 = ((bf16[8,64,512]{2,1,0:T(8,128)(2,1)}), bf16[8,64,512]{2,1,0:T(8,128)(2,1)S(1)}, u32[]{:S(2)}, u32[]{:S(2)}) async-start(bf16[8,64,512]{2,1,0:T(8,128)(2,1)} %broadcast_in_dim.26), calls=%async_computation.8 | async-start | bytes 1048576 | tf_op jit(solution)/shard_map/all_to_all | solution.py:305
  196.2 0.7 copy.75
  197.0 0.3 copy.74
  197.3 1.0 reshape.109
  198.3 0.4 copy.73
  198.7 1.2 reshape.108
  199.9 10.6 %all-to-all-done.8 = bf16[8,64,512]{2,1,0:T(8,128)(2,1)S(1)} async-done(((bf16[8,64,512]{2,1,0:T(8,128)(2,1)}), bf16[8,64,512]{2,1,0:T(8,128)(2,1)S(1)}, u32[]{:S(2)}, u32[]{:S(2)}) %all-to-all-start.8) | async-done | bytes 524320 | tf_op jit(solution)/shard_map/all_to_all | solution.py:305
  210.5 1.0 slice_convert_fusion
  (44 shorter events, 0.7 us)
Async XLA Ops:
  0.6 6.4 %copy-start.6 = (bf16[512,256]{1,0:T(8,128)(2,1)S(1)}, bf16[512,256]{1,0:T(8,128)(2,1)}, u32[]{:S(2)}) copy-start(bf16[512,256]{1,0:T(8,128)(2,1)} %param.17) | copy-start | bytes 786436
  0.6 6.4 %copy-start.7 = (bf16[512,256]{1,0:T(8,128)(2,1)S(1)}, bf16[512,256]{1,0:T(8,128)(2,1)}, u32[]{:S(2)}) copy-start(bf16[512,256]{1,0:T(8,128)(2,1)} %param.18) | copy-start | bytes 786436
  2.7 13.1 %all-to-all-start.1 = ((bf16[4,128,512]{1,2,0:T(8,128)(2,1)}), bf16[4,128,512]{1,2,0:T(8,128)(2,1)S(1)}, u32[]{:S(2)}, u32[]{:S(2)}) async-start(bf16[4,128,512]{1,2,0:T(8,128)(2,1)} %bitcast.10), calls=%async_computation.1 | async-start | bytes 1048576 | tf_op jit(solution)/shard_map/all_to_all | solution.py:305
  7.1 10.2 %copy-start.1 = (bf16[512,512]{1,0:T(8,128)(2,1)}, bf16[512,512]{1,0:T(8,128)(2,1)S(1)}, u32[]{:S(2)}) copy-start(bf16[512,512]{1,0:T(8,128)(2,1)S(1)} %constant_dynamic-update-slice_fusion) | copy-start | bytes 1572868
  16.0 4.7 %copy-start.9 = (bf16[1,128,32]{1,2,0:T(8,128)(2,1)S(1)}, bf16[1,128,32]{1,2,0:T(8,128)(2,1)}, u32[]{:S(2)}) copy-start(bf16[1,128,32]{1,2,0:T(8,128)(2,1)} %param.23) | copy-start | bytes 24580
  16.1 5.0 %copy-start.5 = (bf16[1,128,2048]{2,1,0:T(8,128)(2,1)S(1)}, bf16[1,128,2048]{2,1,0:T(8,128)(2,1)}, u32[]{:S(2)}) copy-start(bf16[1,128,2048]{2,1,0:T(8,128)(2,1)} %param.19) | copy-start | bytes 1572868
  17.3 12.3 %all-to-all-start.2 = ((bf16[4,128,512]{2,1,0:T(8,128)(2,1)}), bf16[4,128,512]{2,1,0:T(8,128)(2,1)S(1)}, u32[]{:S(2)}, u32[]{:S(2)}) async-start(bf16[4,128,512]{2,1,0:T(8,128)(2,1)} %bitcast.13), calls=%async_computation.2 | async-start | bytes 1048576 | tf_op jit(solution)/shard_map/all_to_all | solution.py:305
  29.6 26.4 %all-to-all-start = ((bf16[8,128,384]{2,1,0:T(8,128)(2,1)}), bf16[8,128,384]{2,1,0:T(8,128)(2,1)S(1)}, u32[]{:S(2)}, u32[]{:S(2)}) async-start(bf16[8,128,384]{2,1,0:T(8,128)(2,1)} %fusion.2), calls=%async_computation | async-start | bytes 1572864 | tf_op jit(solution)/shard_map/all_to_all | solution.py:305
  44.4 15.2 %copy-start.13 = (f32[4]{0:T(128)S(1)}, f32[4]{0:T(128)}, u32[]{:S(2)}) copy-start(f32[4]{0:T(128)} %param.30) | copy-start | bytes 52
  44.4 15.4 %copy-start.8 = (f32[1,1024,4]{1,2,0:T(4,128)S(1)}, f32[1,1024,4]{1,2,0:T(4,128)}, u32[]{:S(2)}) copy-start(f32[1,1024,4]{1,2,0:T(4,128)} %param.24) | copy-start | bytes 49156
  56.0 4.0 %copy-start.3 = (bf16[8,128,384]{2,1,0:T(8,128)(2,1)}, bf16[8,128,384]{2,1,0:T(8,128)(2,1)S(1)}, u32[]{:S(2)}) copy-start(bf16[8,128,384]{2,1,0:T(8,128)(2,1)S(1)} %all-to-all-done) | copy-start | bytes 2359300
  56.0 29.4 %all-to-all-start.3 = ((bf16[8,128,512]{2,1,0:T(8,128)(2,1)}), bf16[8,128,512]{2,1,0:T(8,128)(2,1)S(1)}, u32[]{:S(2)}, u32[]{:S(2)}) async-start(bf16[8,128,512]{2,1,0:T(8,128)(2,1)} %pad_maximum_fusion), calls=%async_computation.3 | async-start | bytes 2097152 | tf_op jit(solution)/shard_map/all_to_all | solution.py:305
  59.5 1.3 copy-start.15
  59.6 1.3 copy-start.14
  59.6 1.9 copy-start.10
  59.6 2.5 %copy-start.11 = (f32[5,256]{1,0:T(8,128)S(1)}, f32[5,256]{1,0:T(8,128)}, u32[]{:S(2)}) copy-start(f32[5,256]{1,0:T(8,128)} %param.27) | copy-start | bytes 15364
  59.6 2.5 %copy-start.12 = (f32[5,256]{1,0:T(8,128)S(1)}, f32[5,256]{1,0:T(8,128)}, u32[]{:S(2)}) copy-start(f32[5,256]{1,0:T(8,128)} %param.26) | copy-start | bytes 15364
  85.4 1.0 copy-start
  160.4 4.9 %copy-start.2 = (bf16[512,512]{1,0:T(8,128)(2,1)S(1)}, bf16[512,512]{1,0:T(8,128)(2,1)}, u32[]{:S(2)}) copy-start(bf16[512,512]{1,0:T(8,128)(2,1)} %copy-done.1) | copy-start | bytes 1572868
  161.6 17.9 %all-to-all-start.7 = ((bf16[8,64,512]{2,1,0:T(8,128)(2,1)}), bf16[8,64,512]{2,1,0:T(8,128)(2,1)S(1)}, u32[]{:S(2)}, u32[]{:S(2)}) async-start(bf16[8,64,512]{2,1,0:T(8,128)(2,1)} %bitcast.34), calls=%async_computation.7 | async-start | bytes 1048576 | tf_op jit(solution)/shard_map/all_to_all | solution.py:305
  179.5 12.3 %all-to-all-start.6 = ((bf16[4,128,512]{2,1,0:T(8,128)(2,1)}), bf16[4,128,512]{2,1,0:T(8,128)(2,1)S(1)}, u32[]{:S(2)}, u32[]{:S(2)}) async-start(bf16[4,128,512]{2,1,0:T(8,128)(2,1)} %bitcast.26), calls=%async_computation.6 | async-start | bytes 1048576 | tf_op jit(solution)/shard_map/all_to_all | solution.py:305
  183.0 13.9 %copy-start.4 = (bf16[128,8,256]{2,0,1:T(8,128)(2,1)S(1)}, bf16[128,8,256]{2,0,1:T(8,128)(2,1)}, u32[]{:S(2)}) copy-start(bf16[128,8,256]{2,0,1:T(8,128)(2,1)} %get-tuple-element.10) | copy-start | bytes 1572868
  192.6 17.9 %all-to-all-start.8 = ((bf16[8,64,512]{2,1,0:T(8,128)(2,1)}), bf16[8,64,512]{2,1,0:T(8,128)(2,1)S(1)}, u32[]{:S(2)}, u32[]{:S(2)}) async-start(bf16[8,64,512]{2,1,0:T(8,128)(2,1)} %broadcast_in_dim.26), calls=%async_computation.8 | async-start | bytes 1048576 | tf_op jit(solution)/shard_map/all_to_all | solution.py:305

commit v2 on v1

--- a/solution.py
+++ b/solution.py
@@ -16,6 +16,7 @@
 BLOCK = 128
 INNER = 2048
 LANES = 128
+DT_ROWS = 16
 HALO = 8
 EPSILON = 1e-06
 LOG2E = 1.4426950408889634
@@ -36,35 +37,6 @@
     for odd in (15, 13, 11, 9, 7, 5, 3, 1):
         series = series * z2 + 1.0 / odd
     return jnp.maximum(v, 0.0) + 2.0 * z * series
-
-
-def norm_kernel(values_ref, gates_ref, adjoint_ref, scale_ref, dy_ref, dgate_ref):
-    values = values_ref[...].astype(f32)
-    gates = gates_ref[...].astype(f32)
-    sig = sigmoid(gates)
-    act = gates * sig
-    g = values * act
-    dn = adjoint_ref[...].astype(f32) * scale_ref[...]
-    width = g.shape[1]
-    inv = lax.rsqrt(jnp.sum(g * g, axis=1, keepdims=True) * (1.0 / width) + EPSILON)
-    along = jnp.sum(dn * g, axis=1, keepdims=True) * (1.0 / width)
-    dg = inv * dn - g * (inv * inv * inv * along)
-    dy_ref[...] = (dg * act).astype(bf16)
-    dgate_ref[...] = (dg * values * (sig + act * (1.0 - sig))).astype(bf16)
-
-
-def norm_backward(values, gates, adjoint, scale):
-    tokens, inner = values.shape
-    width = inner // NORM_GROUPS
-    block = pl.BlockSpec((tokens, width), lambda i: (0, i))
-    return pl.pallas_call(
-        norm_kernel,
-        grid=(NORM_GROUPS,),
-        in_specs=[block, block, block, pl.BlockSpec((1, width), lambda i: (0, i))],
-        out_specs=[block, block],
-        out_shape=[jax.ShapeDtypeStruct((tokens, inner), bf16)] * 2,
-        name="norm_backward",
-    )(values, gates, adjoint, scale.reshape(1, inner))
 
 
 def window_conv(padded, r0, taps, flip):
@@ -81,13 +53,17 @@
 def mixer_kernel(
     heads,
     tile,
-    p1_ref,
-    p2_ref,
+    x_ref,
+    dt_ref,
+    dy_ref,
+    bc_ref,
     drop_ref,
     tapx_ref,
     tapbc_ref,
     par_ref,
-    out_ref,
+    dx_ref,
+    dbc_ref,
+    ddt_ref,
     pad_x,
     pad_bc,
     u_ref,
@@ -111,7 +87,7 @@
     rowdl,
     colsum,
 ):
-    window = p1_ref.shape[0]
+    window = x_ref.shape[0]
     xw = u_ref.shape[1]
     chunks = window // BLOCK
     tapx = tapx_ref[...]
@@ -140,13 +116,15 @@
         r0 = pl.multiple_of(c * BLOCK, BLOCK)
         rows = pl.ds(r0, BLOCK)
         into = pl.ds(pl.multiple_of(r0 + HALO, HALO), BLOCK)
-        pad_x[into, :] = p1_ref[rows, :xw].astype(f32)
-        pad_bc[into, :] = p2_ref[rows, xw:].astype(f32)
+        pad_x[into, :] = x_ref[rows, :].astype(f32)
+        pad_bc[into, :] = bc_ref[rows, :].astype(f32)
 
     def prepare(c, carry):
         r0 = pl.multiple_of(c * BLOCK, BLOCK)
         rows = pl.ds(r0, BLOCK)
-        a = p1_ref[rows, xw:].astype(f32) + offset
+        steps = dt_ref[c].astype(f32)
+        steps = jnp.concatenate([steps, jnp.zeros((LANES - DT_ROWS, BLOCK), f32)]).T
+        a = steps + offset
         dt = softplus(a)
         dtc_ref[rows, :] = dt
         sig_ref[rows, :] = sigmoid(a)
@@ -161,7 +139,7 @@
         u_ref[rows, :] = u
         sux_ref[rows, :] = sig + u * (1.0 - sig)
         vt[:, rows] = (u * spread(dt)).T.astype(bf16)
-        dy_t = p2_ref[rows, :xw].astype(f32).T
+        dy_t = dy_ref[rows, :].astype(f32).T
         dyt[:, rows] = dy_t.astype(bf16)
         for h in range(heads):
             dyh[h, rows, :] = dy_t[h * HEAD_DIM : (h + 1) * HEAD_DIM].T.astype(bf16)
@@ -238,8 +216,8 @@
         for h in range(heads):
             along = jnp.sum(jnp.where(lane_head == h, udv, 0.0), axis=1, keepdims=True)
             ddt = ddt + jnp.where(lane == h, along, 0.0)
-        out_ref[rows, xw + 2 * STATE :] = (ddt * sig_ref[rows, :]).astype(bf16)
-        du = dv * spread(dtc_ref[rows, :]) + skip * p2_ref[rows, :xw].astype(f32)
+        ddt_ref[chunks - 1 - i] = (ddt * sig_ref[rows, :]).T[:DT_ROWS].astype(bf16)
+        du = dv * spread(dtc_ref[rows, :]) + skip * dy_ref[rows, :].astype(f32)
         pad_x[into, :] = du * sux_ref[rows, :]
         sbc = sbc_ref[rows, :]
         pad_bc[into, :STATE] = dkt[:, rows].T * sbc[:, :STATE]
@@ -252,12 +230,12 @@
     def _(c):
         r0 = pl.multiple_of(c * BLOCK, BLOCK)
         rows = pl.ds(r0, BLOCK)
-        out_ref[rows, :xw] = window_conv(pad_x, r0, tapx, True).astype(bf16)
-        out_ref[rows, xw : xw + 2 * STATE] = window_conv(pad_bc, r0, tapbc, True).astype(bf16)
-
-
-def mixer_backward(p1, p2, drop, tapx, tapbc, par, heads):
-    window = p1.shape[0]
+        dx_ref[rows, :] = window_conv(pad_x, r0, tapx, True).astype(bf16)
+        dbc_ref[rows, :] = window_conv(pad_bc, r0, tapbc, True).astype(bf16)
+
+
+def mixer_backward(x, dt, dy, bc, drop, tapx, tapbc, par, heads):
+    window = x.shape[0]
     xw = tapx.shape[1]
     tile = 2 * BLOCK if window % (2 * BLOCK) == 0 else BLOCK
     rows_h = -(-heads // 8) * 8
@@ -287,13 +265,17 @@
     ]
     return pl.pallas_call(
         functools.partial(mixer_kernel, heads, tile),
-        in_specs=[pl.BlockSpec(memory_space=pltpu.VMEM)] * 6,
-        out_specs=pl.BlockSpec(memory_space=pltpu.VMEM),
-        out_shape=jax.ShapeDtypeStruct((window, xw + 2 * STATE + LANES), bf16),
+        in_specs=[pl.BlockSpec(memory_space=pltpu.VMEM)] * 8,
+        out_specs=[pl.BlockSpec(memory_space=pltpu.VMEM)] * 3,
+        out_shape=[
+            jax.ShapeDtypeStruct((window, xw), bf16),
+            jax.ShapeDtypeStruct((window, 2 * STATE), bf16),
+            jax.ShapeDtypeStruct(dt.shape, bf16),
+        ],
         scratch_shapes=scratch,
         compiler_params=pltpu.CompilerParams(vmem_limit_bytes=62 * 1024 * 1024),
         name="mixer_backward",
-    )(p1, p2, drop, tapx, tapbc, par)
+    )(x, dt, dy, bc, drop, tapx, tapbc, par)
 
 
 def pad_last(values, width):
@@ -301,13 +283,270 @@
     return jnp.pad(values, pads)
 
 
-def exchange(values, axis):
-    return lax.all_to_all(values, axis, split_axis=0, concat_axis=0, tiled=True)
-
-
 def by_owner(values, owners):
     tokens, width = values.shape
     return jnp.transpose(values.reshape(tokens, owners, width // owners), (1, 0, 2))
+
+
+def greet(axes):
+    barrier = pltpu.get_barrier_semaphore()
+    count = 0
+    for axis in axes:
+        size = lax.axis_size(axis)
+        me = lax.axis_index(axis)
+        for o in range(1, size):
+            pl.semaphore_signal(
+                barrier,
+                inc=1,
+                device_id={axis: lax.rem(me + o, size)},
+                device_id_type=pl.DeviceIdType.MESH,
+            )
+            count += 1
+    pl.semaphore_wait(barrier, count)
+
+
+def send_all(axis, source, target, sems, slot):
+    size = lax.axis_size(axis)
+    me = lax.axis_index(axis)
+    copies = []
+    for o in range(1, size):
+        peer = lax.rem(me + o, size)
+        copies.append(
+            pltpu.make_async_remote_copy(
+                src_ref=source(peer),
+                dst_ref=target(me),
+                send_sem=sems.at[slot, 0, o],
+                recv_sem=sems.at[slot, 1, o],
+                device_id={axis: peer},
+                device_id_type=pl.DeviceIdType.MESH,
+            )
+        )
+    for copy in copies:
+        copy.start()
+    return copies
+
+
+def received(copies):
+    for copy in copies:
+        copy.wait_recv()
+
+
+def lanes_of(index, width):
+    return pl.ds(pl.multiple_of(index * width, LANES), width)
+
+
+def front_kernel(
+    heads,
+    la_ref,
+    w_ref,
+    x_ref,
+    dt_ref,
+    values_ref,
+    gates_ref,
+    adjoint_ref,
+    scale_ref,
+    cols_ref,
+    xall_ref,
+    dtall_ref,
+    dyall_ref,
+    bcall_ref,
+    dgate_ref,
+    dysend,
+    psend,
+    pall,
+    bcsend,
+    sems,
+):
+    dp = lax.axis_size("dp")
+    sp = lax.axis_size("sp")
+    me_dp = lax.axis_index("dp")
+    me_sp = lax.axis_index("sp")
+    tokens, width_in = la_ref.shape
+    cw = width_in // dp
+    xc = heads * HEAD_DIM
+    per_group = HEADS // GROUPS
+    greet(("dp", "sp"))
+    la_copies = send_all(
+        "dp", lambda p: la_ref.at[:, lanes_of(p, cw)], lambda m: cols_ref.at[m], sems, 0
+    )
+    x_copies = send_all("sp", lambda p: x_ref.at[p], lambda m: xall_ref.at[m], sems, 1)
+    dt_copies = send_all("sp", lambda p: dt_ref.at[p], lambda m: dtall_ref.at[m], sems, 2)
+    cols_ref[me_dp] = la_ref[:, lanes_of(me_dp, cw)]
+    xall_ref[me_sp] = x_ref[me_sp]
+    dtall_ref[me_sp] = dt_ref[me_sp]
+
+    inner = values_ref.shape[1]
+    width = inner // NORM_GROUPS
+    for group in range(NORM_GROUPS):
+        span = slice(group * width, (group + 1) * width)
+        values = values_ref[:, span].astype(f32)
+        gates = gates_ref[:, span].astype(f32)
+        sig = sigmoid(gates)
+        act = gates * sig
+        g = values * act
+        dn = adjoint_ref[:, span].astype(f32) * scale_ref[:, span]
+        inv = lax.rsqrt(jnp.sum(g * g, axis=1, keepdims=True) * (1.0 / width) + EPSILON)
+        along = jnp.sum(dn * g, axis=1, keepdims=True) * (1.0 / width)
+        dg = inv * dn - g * (inv * inv * inv * along)
+        dgate_ref[:, span] = (dg * values * (sig + act * (1.0 - sig))).astype(bf16)
+        dy = (dg * act).astype(bf16)
+        step = min(width, xc)
+        for part in range(width // step):
+            at = group * width + part * step
+            owner, first = at // xc, at % xc
+            dysend[owner, :, first : first + step] = dy[:, part * step : (part + 1) * step]
+            if xc < dysend.shape[2]:
+                dysend[owner, :, xc:] = jnp.zeros((tokens, dysend.shape[2] - xc), bf16)
+    dy_copies = send_all("sp", lambda p: dysend.at[p], lambda m: dyall_ref.at[m], sems, 3)
+    dyall_ref[me_sp] = dysend[me_sp]
+
+    received(la_copies)
+    for i in range(dp):
+        psend[i] = jnp.dot(cols_ref[i], w_ref[...], preferred_element_type=f32).astype(bf16)
+    p_copies = send_all("dp", lambda p: psend.at[p], lambda m: pall.at[m], sems, 4)
+    total = psend[me_dp].astype(f32)
+    pall[me_dp] = jnp.zeros(pall.shape[1:], bf16)
+    received(p_copies)
+    for i in range(dp):
+        total = total + pall[i].astype(f32)
+    total = total.astype(bf16)
+    for group in range(GROUPS):
+        at = group * STATE
+        bcsend[group, :, :STATE] = total[:, at : at + STATE]
+        at = (GROUPS + group) * STATE
+        bcsend[group, :, STATE:] = total[:, at : at + STATE]
+    bc_copies = send_all(
+        "sp",
+        lambda p: bcsend.at[(p * heads) // per_group],
+        lambda m: bcall_ref.at[m],
+        sems,
+        5,
+    )
+    bcall_ref[me_sp] = bcsend[(me_sp * heads) // per_group]
+    for copies in (x_copies, dt_copies, dy_copies, bc_copies):
+        received(copies)
+    for copies in (la_copies, x_copies, dt_copies, dy_copies, p_copies, bc_copies):
+        for copy in copies:
+            copy.wait_send()
+
+
+def back_kernel(
+    heads,
+    dx_ref,
+    dbc_ref,
+    ddt_ref,
+    cols_ref,
+    w_ref,
+    dxout_ref,
+    ddtout_ref,
+    dh_ref,
+    dwb_ref,
+    dwc_ref,
+    dbcall,
+    gall,
+    gsend,
+    wsend,
+    wall,
+    hsend,
+    ssend,
+    tall,
+    sems,
+):
+    dp = lax.axis_size("dp")
+    sp = lax.axis_size("sp")
+    me_dp = lax.axis_index("dp")
+    me_sp = lax.axis_index("sp")
+    tokens = dx_ref.shape[1]
+    cw = w_ref.shape[0]
+    xc = heads * HEAD_DIM
+    latent = GROUPS * STATE
+    direct = xc % LANES == 0
+    rows = cw // sp
+    greet(("dp", "sp"))
+    dbc_copies = send_all("sp", lambda p: dbc_ref.at[p], lambda m: dbcall.at[m], sems, 0)
+    if direct:
+        dx_to = lambda m: dxout_ref.at[:, lanes_of(m, xc)]
+    else:
+        dx_to = lambda m: dxout_ref.at[m]
+    dx_copies = send_all("sp", lambda p: dx_ref.at[p], dx_to, sems, 1)
+    ddt_copies = send_all("sp", lambda p: ddt_ref.at[p], lambda m: ddtout_ref.at[m], sems, 2)
+    dbcall[me_sp] = dbc_ref[me_sp]
+    ddtout_ref[me_sp] = ddt_ref[me_sp]
+    if direct:
+        dxout_ref[:, lanes_of(me_sp, xc)] = dx_ref[me_sp]
+    else:
+        dxout_ref[me_sp] = dx_ref[me_sp]
+    received(dbc_copies)
+    members = sp // GROUPS
+    for group in range(GROUPS):
+        total = dbcall[group * members].astype(f32)
+        for member in range(1, members):
+            total = total + dbcall[group * members + member].astype(f32)
+        total = total.astype(bf16)
+        at = group * STATE
+        gsend[:, at : at + STATE] = total[:, :STATE]
+        at = (GROUPS + group) * STATE
+        gsend[:, at : at + STATE] = total[:, STATE:]
+    g_copies = send_all("dp", lambda p: gsend, lambda m: gall.at[m], sems, 3)
+    gall[me_dp] = gsend[...]
+    received(g_copies)
+    total = None
+    for i in range(dp):
+        term = lax.dot_general(
+            cols_ref[i], gall[i], (((0,), (0,)), ((), ())), preferred_element_type=f32
+        )
+        total = term if total is None else total + term
+    wsend[...] = total.astype(bf16).reshape(sp, rows, 2 * latent)
+    w_copies = send_all("sp", lambda p: wsend.at[p], lambda m: wall.at[m], sems, 4)
+    wall[me_sp] = wsend[me_sp]
+    for i in range(dp):
+        hsend[i] = lax.dot_general(
+            gall[i], w_ref[...], (((1,), (1,)), ((), ())), preferred_element_type=f32
+        ).astype(bf16)
+    h_copies = send_all(
+        "dp", lambda p: hsend.at[p], lambda m: dh_ref.at[:, lanes_of(m, cw)], sems, 5
+    )
+    dh_ref[:, lanes_of(me_dp, cw)] = hsend[me_dp]
+    received(w_copies)
+    share = wall[0].astype(f32)
+    for j in range(1, sp):
+        share = share + wall[j].astype(f32)
+    ssend[...] = share.astype(bf16)
+    s_copies = send_all("sp", lambda p: ssend, lambda m: tall.at[m], sems, 6)
+    tall[me_sp] = ssend[...]
+    received(s_copies)
+    for j in range(sp):
+        dwb_ref[j] = tall[j, :, :latent].astype(f32)
+        dwc_ref[j] = tall[j, :, latent:].astype(f32)
+    for copies in (dx_copies, ddt_copies, h_copies):
+        received(copies)
+    for copies in (
+        dbc_copies,
+        dx_copies,
+        ddt_copies,
+        g_copies,
+        w_copies,
+        h_copies,
+        s_copies,
+    ):
+        for copy in copies:
+            copy.wait_send()
+
+
+def comm_call(kernel, args, shapes, scratch, slots, peers, number, name):
+    vmem = pl.BlockSpec(memory_space=pltpu.VMEM)
+    return pl.pallas_call(
+        kernel,
+        in_specs=[vmem] * len(args),
+        out_specs=[vmem] * len(shapes),
+        out_shape=[jax.ShapeDtypeStruct(shape, kind) for shape, kind in shapes],
+        scratch_shapes=[pltpu.VMEM(shape, bf16) for shape in scratch]
+        + [pltpu.SemaphoreType.DMA((slots, 2, peers))],
+        compiler_params=pltpu.CompilerParams(
+            collective_id=number, has_side_effects=True, vmem_limit_bytes=60 * 1024 * 1024
+        ),
+        name=name,
+    )(*args)
 
 
 def local(
@@ -338,35 +577,43 @@
     xc = heads * HEAD_DIM
     xw = -(-xc // LANES) * LANES
     window = tokens * sp
-
-    columns = exchange(by_owner(layer_activity.reshape(tokens, width_in), dp), "dp")
-    columns = columns.reshape(dp * tokens, width_in // dp)
+    cw = width_in // dp
+    peers = max(sp, dp)
+
     weights = jnp.concatenate([writer_matrix, reader_matrix], axis=1)
-    partial = jnp.dot(columns, weights, preferred_element_type=f32).astype(bf16)
-    p1 = exchange(
-        jnp.concatenate(
-            [
-                pad_last(by_owner(source_unfiltered.reshape(tokens, INNER), sp), xw),
-                pad_last(by_owner(delta_raw.reshape(tokens, HEADS), sp), LANES),
-            ],
-            axis=2,
+    x_by = pad_last(by_owner(source_unfiltered.reshape(tokens, INNER), sp), xw)
+    dt_by = delta_raw.reshape(tokens, HEADS).T.reshape(sp, heads, tokens)
+    dt_by = jnp.pad(dt_by, ((0, 0), (0, DT_ROWS - heads), (0, 0)))
+    cols, x_all, dt_all, dy_all, bc_all, d_gate = comm_call(
+        functools.partial(front_kernel, heads),
+        (
+            layer_activity.reshape(tokens, width_in),
+            weights,
+            x_by,
+            dt_by,
+            saved_result.reshape(tokens, INNER),
+            switch_raw_signal.reshape(tokens, INNER),
+            final_adjoint.reshape(tokens, INNER),
+            rescale_factor.reshape(1, INNER),
         ),
-        "sp",
-    )
-    result_adjoint, d_gate = norm_backward(
-        saved_result.reshape(tokens, INNER),
-        switch_raw_signal.reshape(tokens, INNER),
-        final_adjoint.reshape(tokens, INNER),
-        rescale_factor,
-    )
-    partial = exchange(partial.reshape(dp, tokens, 2 * latent), "dp")
-    projected = jnp.sum(partial.astype(f32), axis=0).astype(bf16)
-    maps = jnp.transpose(projected.reshape(tokens, 2, GROUPS, STATE), (2, 0, 1, 3))
-    maps = jnp.broadcast_to(
-        maps.reshape(GROUPS, 1, tokens, 2 * STATE), (GROUPS, sp // GROUPS, tokens, 2 * STATE)
-    ).reshape(sp, tokens, 2 * STATE)
-    p2 = exchange(
-        jnp.concatenate([pad_last(by_owner(result_adjoint, sp), xw), maps], axis=2), "sp"
+        (
+            ((dp, tokens, cw), bf16),
+            ((sp, tokens, xw), bf16),
+            ((sp, DT_ROWS, tokens), bf16),
+            ((sp, tokens, xw), bf16),
+            ((sp, tokens, 2 * STATE), bf16),
+            ((tokens, INNER), bf16),
+        ),
+        (
+            (sp, tokens, xw),
+            (dp, tokens, 2 * latent),
+            (dp, tokens, 2 * latent),
+            (GROUPS, tokens, 2 * STATE),
+        ),
+        6,
+        peers,
+        0,
+        "front",
     )
 
     group = lax.axis_index("sp") * heads // per_group
@@ -378,9 +625,11 @@
         axis=1,
     )
     par = pad_last(jnp.stack([delta_offset, jnp.exp(fading_exponents)]), LANES)
-    back = mixer_backward(
-        p1.reshape(window, xw + LANES),
-        p2.reshape(window, xw + 2 * STATE),
+    dx, dbc, ddt = mixer_backward(
+        x_all.reshape(window, xw),
+        dt_all,
+        dy_all.reshape(window, xw),
+        bc_all.reshape(window, 2 * STATE),
         pad_last(extra_logdrop.reshape(window, heads), LANES),
         pad_last(
             jnp.concatenate([source_filter_coefs, jnp.repeat(direct_factor, HEAD_DIM)[None]]), xw
@@ -389,38 +638,48 @@
         par,
         heads,
     )
-    back = exchange(back.reshape(sp, tokens, xw + 2 * STATE + LANES), "sp")
-    back_x = jnp.transpose(back[:, :, :xc], (1, 0, 2)).reshape(1, tokens, INNER)
-    back_dt = jnp.transpose(
-        back[:, :, xw + 2 * STATE : xw + 2 * STATE + heads], (1, 0, 2)
-    ).reshape(1, tokens, HEADS)
-    summed = jnp.sum(
-        back[:, :, xw : xw + 2 * STATE]
-        .astype(f32)
-        .reshape(GROUPS, sp // GROUPS, tokens, 2, STATE),
-        axis=1,
-    )
-    gradients = jnp.transpose(summed, (1, 2, 0, 3)).reshape(tokens, 2 * latent).astype(bf16)
-    all_grads = exchange(
-        jnp.broadcast_to(gradients[None], (dp, tokens, 2 * latent)), "dp"
-    ).reshape(dp * tokens, 2 * latent)
-    rows = width_in // dp
-    local_rows = jnp.einsum("td,tc->dc", columns, all_grads, preferred_element_type=f32)
-    shares = exchange(local_rows.astype(bf16).reshape(sp, rows // sp, 2 * latent), "sp")
-    share = jnp.sum(shares.astype(f32), axis=0).astype(bf16)
-    total_grad = exchange(
-        jnp.broadcast_to(share[None], (sp, rows // sp, 2 * latent)), "sp"
-    ).reshape(rows, 2 * latent)
-    d_cols = jnp.einsum("tc,dc->td", all_grads, weights, preferred_element_type=f32)
-    d_hidden = exchange(d_cols.astype(bf16).reshape(dp, tokens, rows), "dp")
-    d_hidden = jnp.transpose(d_hidden, (1, 0, 2)).reshape(1, tokens, width_in)
+    rows = cw // sp
+    back_x, back_dt, d_hidden, d_w_b, d_w_c = comm_call(
+        functools.partial(back_kernel, heads),
+        (
+            dx.reshape(sp, tokens, xw),
+            dbc.reshape(sp, tokens, 2 * STATE),
+            ddt,
+            cols,
+            weights,
+        ),
+        (
+            ((tokens, INNER) if xc % LANES == 0 else (sp, tokens, xw), bf16),
+            ((sp, DT_ROWS, tokens), bf16),
+            ((tokens, width_in), bf16),
+            ((sp, rows, latent), f32),
+            ((sp, rows, latent), f32),
+        ),
+        (
+            (sp, tokens, 2 * STATE),
+            (dp, tokens, 2 * latent),
+            (tokens, 2 * latent),
+            (sp, rows, 2 * latent),
+            (sp, rows, 2 * latent),
+            (dp, tokens, cw),
+            (rows, 2 * latent),
+            (sp, rows, 2 * latent),
+        ),
+        7,
+        peers,
+        1,
+        "back",
+    )
+    if xc % LANES:
+        back_x = jnp.transpose(back_x[:, :, :xc], (1, 0, 2))
+    back_dt = back_dt[:, :heads].reshape(HEADS, tokens).T
     return (
-        d_hidden,
-        back_x,
+        d_hidden.reshape(1, tokens, width_in),
+        back_x.reshape(1, tokens, INNER),
         d_gate.reshape(1, tokens, INNER),
-        back_dt,
-        total_grad[:, :latent].astype(f32),
-        total_grad[:, latent:].astype(f32),
+        back_dt.reshape(1, tokens, HEADS),
+        d_w_b.reshape(cw, latent),
+        d_w_c.reshape(cw, latent),
     )
 
 

time: 213 us -> 142 us (0.67)
  Pallas kernels: 31.4 us -> 124 us
  waiting for transfers between devices: 82.6 us -> 0 us
  blocking collectives: 46.4 us -> 0 us
  starting transfers between devices: 28.5 us -> 0 us
  other arithmetic: 5.76 us -> 1.73 us
  matrix products: 3.73 us -> 0 us
    pallas_call x1 -> x2, Pallas kernels: 5.82 us -> 97.9 us  [comm_call(): pl.pallas_call(kernel, in_specs=[vmem] * len(args), out_specs=[vmem] * le...]
    all_to_all x7 -> x0, waiting for transfers between devices: 82.6 us -> none  [exchange(): return lax.all_to_all(values, axis, split_axis=0, concat_axis=0, tiled=True)]
    all_to_all x2 -> x0, blocking collectives: 46.4 us -> none  [exchange(): return lax.all_to_all(values, axis, split_axis=0, concat_axis=0, tiled=True)]
    all_to_all x7 -> x0, starting transfers between devices: 28.5 us -> none  [exchange(): return lax.all_to_all(values, axis, split_axis=0, concat_axis=0, tiled=True)]
    unnamed x36 -> x38, local copies, waits for them, and re-layouts: 3.49 us -> 9.53 us
    dot_general x3 -> x0, matrix products: 3.73 us -> none  [the longest x1 1.27 us: local(): jnp.einsum('tc,dc->td', all_grads, weights, preferred_element_type=f32)]
    reshape x4 -> x0, local copies, waits for them, and re-layouts: 3.4 us -> none  [the longest x1 1.17 us: local(): d_hidden = jnp.transpose(d_hidden, (1, 0, 2)).reshape(1, tokens, width_in)]
    transpose x6 -> x0, local copies, waits for them, and re-layouts: 2.41 us -> none  [the longest x2 1.2 us: local(): back_x = jnp.transpose(back[:, :, :xc], (1, 0, 2)).reshape(1, tokens, INNER)]
  transfers between devices with their start and end apart: 7 -> 0, of which waited for: 7 -> 0; matrix products, arithmetic and copies ran while one was open for 6% -> 0% of each run, Pallas kernels for 3% -> 0%
where the time goes in v2:
time: 142 us; the launch traced here: 140 us
  Pallas kernels  124 us (87%)
  local copies, waits for them, and re-layouts  13.5 us (10%)
  other arithmetic  1.73 us (1%)
    pallas_call x2, Pallas kernels, comm_call(): pl.pallas_call(kernel, in_specs=[vmem] * len(args), out_specs=[vmem] * le...  97.9 us
    pallas_call x1, Pallas kernels, mixer_backward(): pl.pallas_call(functools.partial(mixer_kernel, heads, tile), in_specs=[pl...  26.3 us
    unnamed x38, local copies, waits for them, and re-layouts  9.53 us

profile of v2, /device:TPU:0, one launch (start us, length us, event | category | flops | bytes accessed | tf_op | source)
XLA Modules:
  0.0 140.2 jit_solution(3912675385528368304)
XLA Ops:
  0.7 0.0 copy-start.14
  0.7 0.0 copy-start.13
  0.7 0.0 copy-start.8
  0.7 0.6 copy-done.14
  1.3 0.0 copy-done.13
  1.3 0.0 copy-start.12
  1.3 0.5 select_maximum_fusion.par_ref
  1.9 0.1 copy-done.12
  2.0 0.1 broadcast_in_dim.3
  2.1 0.1 broadcast_in_dim_reshape.3
  2.1 0.0 copy-done.8
  2.1 0.0 copy-start.11
  2.1 0.6 pad_maximum_fusion.tapx_ref
  2.7 0.1 copy-done.10
  2.8 0.0 copy-done.11
  2.9 0.0 copy-start.9
  2.9 0.6 pad_maximum_fusion.1.tapbc_ref
  3.5 0.1 copy-done.9
  3.6 0.0 copy-start.6
  3.6 0.6 pad.12.dt_ref
  4.2 0.0 copy-start.1
  4.2 1.0 constant_dynamic-update-slice_fusion.1
  5.2 0.0 copy-done.6
  5.3 0.1 copy-done.1
  5.3 0.0 copy-start
  5.3 0.3 copy.23
  5.6 0.5 copy-done
  6.1 0.0 copy-start.7
  6.1 1.0 copy.24
  7.1 0.0 copy-done.7
  7.1 0.2 copy.25
  7.4 0.8 pad.13.drop_ref
  8.2 42.7 %front.1 = (bf16[4,128,512]{2,1,0:T(8,128)(2,1)}, bf16[8,128,256]{2,1,0:T(8,128)(2,1)}, bf16[8,16,128]{2,1,0:T(8,128)(2,1)}, bf16[8,128,256]{2,1,0:T(8,128)(2,1)...) custom-call(bf16[128,2048]{1,0:T(8,128)(2,1)} %bitcast.34, bf16[512,512]{1,0:T(8,128)(2,1)} %copy-done, ...), custom_call_target="tpu_custom_call" | custom-call | tf_op jit(solution)/shard_map/front/pallas_call | solution.py:538
  50.9 26.3 %mixer_backward.1 = (bf16[1024,256]{1,0:T(8,128)(2,1)}, bf16[1024,256]{1,0:T(8,128)(2,1)}, bf16[8,16,128]{2,1,0:T(8,128)(2,1)}) custom-call(bf16[1024,256]{1,0:T(8,128)(2,1)} %bitcast.45, bf16[8,16,128]{2,1,0:T(8,128)(2,1)} %get-tuple-element.21.dt_ref, bf16[1024,256]{1,0:T(8,128)(2,1)} %bitcast.46, bf16[1024,256]{1,0:T(8,128)(2,1)} %bitcast.47, ...), custom_call_target="tpu_custom_call" | custom-call | tf_op jit(solution)/shard_map/mixer_backward/pallas_call | solution.py:266
  77.2 55.2 %back.1 = (bf16[128,2048]{1,0:T(8,128)(2,1)}, bf16[8,16,128]{2,1,0:T(8,128)(2,1)}, bf16[128,2048]{1,0:T(8,128)(2,1)}, f32[8,64,256]{2,1,0:T(8,128)}, f32[8,64,256]{2,1,0:T(8,128)}) custom-call(bf16[8,128,256]{2,1,0:T(8,128)(2,1)} %bitcast.43, bf16[8,128,256]{2,1,0:T(8,128)(2,1)} %bitcast.44, bf16[8,16,128]{2,1,0:T(8,128)(2,1)} %get-tuple-element.26.ddt_ref, ...), custom_call_target="tpu_custom_call" | custom-call | tf_op jit(solution)/shard_map/back/pallas_call | solution.py:538
  132.4 1.3 slice.3
  133.7 0.0 copy-start.5
  133.7 1.9 %copy.32 = bf16[1,128,2048]{2,1,0:T(8,128)(2,1)} copy(bf16[1,128,2048]{2,1,0:T(8,128)(2,1)} %bitcast.42) | data formatting | bytes 1048576
  135.7 0.0 copy-done.5
  135.7 0.0 copy-start.2
  135.7 0.8 copy.33
  136.5 0.4 copy-done.2
  136.9 0.0 copy-start.4
  136.9 0.8 copy.34
  137.7 0.4 copy-done.4
  138.1 0.8 copy.35
  138.9 0.4 copy-done.3
  139.4 0.8 copy.36
  (5 shorter events, 0.0 us)
Async XLA Ops:
  0.7 0.7 copy-start.14
  0.7 0.7 copy-start.13
  0.7 1.5 %copy-start.8 = (f32[5,256]{1,0:T(8,128)S(1)}, f32[5,256]{1,0:T(8,128)}, u32[]{:S(2)}) copy-start(f32[5,256]{1,0:T(8,128)} %param.25) | copy-start | bytes 15364
  1.3 0.7 copy-start.12
  2.1 0.7 copy-start.10
  2.1 0.7 copy-start.11
  2.9 0.7 copy-start.9
  3.6 1.7 %copy-start.6 = (bf16[512,256]{1,0:T(8,128)(2,1)S(1)}, bf16[512,256]{1,0:T(8,128)(2,1)}, u32[]{:S(2)}) copy-start(bf16[512,256]{1,0:T(8,128)(2,1)} %param.18) | copy-start | bytes 786436
  4.2 1.1 copy-start.1
  5.3 0.8 copy-start
  6.1 1.0 copy-start.7
  133.7 1.9 %copy-start.5 = (bf16[128,2048]{1,0:T(8,128)(2,1)S(1)}, bf16[128,2048]{1,0:T(8,128)(2,1)}, u32[]{:S(2)}) copy-start(bf16[128,2048]{1,0:T(8,128)(2,1)} %get-tuple-element.29) | copy-start | bytes 1572868
  135.7 1.2 copy-start.2
  136.9 1.2 copy-start.4
  138.1 1.2 copy-start.3

commit v3 on v2

--- a/solution.py
+++ b/solution.py
@@ -468,8 +468,6 @@
         dx_to = lambda m: dxout_ref.at[:, lanes_of(m, xc)]
     else:
         dx_to = lambda m: dxout_ref.at[m]
-    dx_copies = send_all("sp", lambda p: dx_ref.at[p], dx_to, sems, 1)
-    ddt_copies = send_all("sp", lambda p: ddt_ref.at[p], lambda m: ddtout_ref.at[m], sems, 2)
     dbcall[me_sp] = dbc_ref[me_sp]
     ddtout_ref[me_sp] = ddt_ref[me_sp]
     if direct:
@@ -488,6 +486,8 @@
         at = (GROUPS + group) * STATE
         gsend[:, at : at + STATE] = total[:, STATE:]
     g_copies = send_all("dp", lambda p: gsend, lambda m: gall.at[m], sems, 3)
+    dx_copies = send_all("sp", lambda p: dx_ref.at[p], dx_to, sems, 1)
+    ddt_copies = send_all("sp", lambda p: ddt_ref.at[p], lambda m: ddtout_ref.at[m], sems, 2)
     gall[me_dp] = gsend[...]
     received(g_copies)
     total = None

time: 142 us -> 142 us (level)
  Pallas kernels: 124 us -> 126 us
where the time goes in v3:
time: 142 us
  Pallas kernels  126 us (89%)
  local copies, waits for them, and re-layouts  13.5 us (10%)
  other arithmetic  1.73 us (1%)
    pallas_call x2, Pallas kernels, comm_call(): pl.pallas_call(kernel, in_specs=[vmem] * len(args), out_specs=[vmem] * le...  99.2 us
    pallas_call x1, Pallas kernels, mixer_backward(): pl.pallas_call(functools.partial(mixer_kernel, heads, tile), in_specs=[pl...  26.3 us
    unnamed x38, local copies, waits for them, and re-layouts  9.53 us

profile of v3, /device:TPU:0, one launch (start us, length us, event | category | flops | bytes accessed | tf_op | source)
XLA Modules:
  0.0 141.5 jit_solution(4370546662378754657)
XLA Ops:
  0.7 0.0 copy-start.14
  0.7 0.0 copy-start.13
  0.7 0.0 copy-start.8
  0.7 0.6 copy-done.14
  1.3 0.0 copy-done.13
  1.3 0.0 copy-start.12
  1.3 0.5 select_maximum_fusion.par_ref
  1.9 0.1 copy-done.12
  2.0 0.1 broadcast_in_dim.3
  2.1 0.1 broadcast_in_dim_reshape.3
  2.1 0.0 copy-done.8
  2.1 0.0 copy-start.10
  2.1 0.0 copy-start.11
  2.1 0.6 pad_maximum_fusion.tapx_ref
  2.7 0.1 copy-done.10
  2.8 0.0 copy-done.11
  2.9 0.0 copy-start.9
  2.9 0.6 pad_maximum_fusion.1.tapbc_ref
  3.5 0.1 copy-done.9
  3.6 0.0 copy-start.6
  3.6 0.6 pad.12.dt_ref
  4.2 0.0 copy-start.1
  4.2 1.0 constant_dynamic-update-slice_fusion.1
  5.2 0.0 copy-done.6
  5.3 0.1 copy-done.1
  5.3 0.0 copy-start
  5.3 0.3 copy.23
  5.6 0.5 copy-done
  6.1 0.0 copy-start.7
  6.1 1.0 copy.24
  7.1 0.0 copy-done.7
  7.1 0.2 copy.25
  7.4 0.8 pad.13.drop_ref
  8.2 42.7 %front.1 = (bf16[4,128,512]{2,1,0:T(8,128)(2,1)}, bf16[8,128,256]{2,1,0:T(8,128)(2,1)}, bf16[8,16,128]{2,1,0:T(8,128)(2,1)}, bf16[8,128,256]{2,1,0:T(8,128)(2,1)...) custom-call(bf16[128,2048]{1,0:T(8,128)(2,1)} %bitcast.34, bf16[512,512]{1,0:T(8,128)(2,1)} %copy-done, ...), custom_call_target="tpu_custom_call" | custom-call | tf_op jit(solution)/shard_map/front/pallas_call | solution.py:538
  50.9 26.3 %mixer_backward.1 = (bf16[1024,256]{1,0:T(8,128)(2,1)}, bf16[1024,256]{1,0:T(8,128)(2,1)}, bf16[8,16,128]{2,1,0:T(8,128)(2,1)}) custom-call(bf16[1024,256]{1,0:T(8,128)(2,1)} %bitcast.45, bf16[8,16,128]{2,1,0:T(8,128)(2,1)} %get-tuple-element.21.dt_ref, bf16[1024,256]{1,0:T(8,128)(2,1)} %bitcast.46, bf16[1024,256]{1,0:T(8,128)(2,1)} %bitcast.47, ...), custom_call_target="tpu_custom_call" | custom-call | tf_op jit(solution)/shard_map/mixer_backward/pallas_call | solution.py:266
  77.2 56.6 %back.1 = (bf16[128,2048]{1,0:T(8,128)(2,1)}, bf16[8,16,128]{2,1,0:T(8,128)(2,1)}, bf16[128,2048]{1,0:T(8,128)(2,1)}, f32[8,64,256]{2,1,0:T(8,128)}, f32[8,64,256]{2,1,0:T(8,128)}) custom-call(bf16[8,128,256]{2,1,0:T(8,128)(2,1)} %bitcast.43, bf16[8,128,256]{2,1,0:T(8,128)(2,1)} %bitcast.44, bf16[8,16,128]{2,1,0:T(8,128)(2,1)} %get-tuple-element.26.ddt_ref, ...), custom_call_target="tpu_custom_call" | custom-call | tf_op jit(solution)/shard_map/back/pallas_call | solution.py:538
  133.8 1.3 slice.3
  135.1 0.0 copy-start.5
  135.1 1.9 %copy.32 = bf16[1,128,2048]{2,1,0:T(8,128)(2,1)} copy(bf16[1,128,2048]{2,1,0:T(8,128)(2,1)} %bitcast.42) | data formatting | bytes 1048576
  137.0 0.0 copy-done.5
  137.0 0.0 copy-start.2
  137.0 0.8 copy.33
  137.8 0.4 copy-done.2
  138.3 0.8 copy.34
  139.0 0.4 copy-done.4
  139.5 0.8 copy.35
  140.3 0.4 copy-done.3
  140.7 0.8 copy.36
  (5 shorter events, 0.0 us)
Async XLA Ops:
  0.7 0.7 copy-start.14
  0.7 0.7 copy-start.13
  0.7 1.5 %copy-start.8 = (f32[5,256]{1,0:T(8,128)S(1)}, f32[5,256]{1,0:T(8,128)}, u32[]{:S(2)}) copy-start(f32[5,256]{1,0:T(8,128)} %param.25) | copy-start | bytes 15364
  1.3 0.7 copy-start.12
  2.1 0.7 copy-start.10
  2.1 0.7 copy-start.11
  2.9 0.7 copy-start.9
  3.6 1.7 %copy-start.6 = (bf16[512,256]{1,0:T(8,128)(2,1)S(1)}, bf16[512,256]{1,0:T(8,128)(2,1)}, u32[]{:S(2)}) copy-start(bf16[512,256]{1,0:T(8,128)(2,1)} %param.18) | copy-start | bytes 786436
  4.2 1.1 copy-start.1
  5.3 0.8 copy-start
  6.1 1.0 copy-start.7
  135.1 1.9 %copy-start.5 = (bf16[128,2048]{1,0:T(8,128)(2,1)S(1)}, bf16[128,2048]{1,0:T(8,128)(2,1)}, u32[]{:S(2)}) copy-start(bf16[128,2048]{1,0:T(8,128)(2,1)} %get-tuple-element.29) | copy-start | bytes 1572868
  137.0 1.2 copy-start.2
  138.3 1.2 copy-start.4
  139.5 1.2 copy-start.3
